TPU v7x, 32 devices: a whole 2x2x4 slice. The times are simulated.
32 devices in a mesh: grp: 2 (over x), row: 4 (over z), col: 4 (over y, core).
Axes of the slice: x: 2, y: 2, z: 4, core: 2. Of those that a mesh axis runs over, the one named last changes fastest.
Arguments:
- tokens: bfloat16 [2, 2048, 2048], P('grp', ('row', 'col')), parts along dimension 0, may hold values from -6 to 6
- norm_gain: bfloat16 [2048], replicated, may hold values from 0.099609375 to 1.8984375
- w_in: bfloat16 [2048, 512], replicated, may hold values from -0.125 to 0.125
- w_out: bfloat16 [512, 2048], replicated, may hold values from -0.25 to 0.25
Outputs:
- mixed: bfloat16 [2, 2048, 2048], P('grp', ('row', 'col')), parts along dimension 0
There are 2 independent parts, one for each index of `grp`. A program takes and returns all parts, laid end to end along the dimension named above; an argument that names none is the same for every part. Nothing has to cross between parts.
All inputs are finite; a program needn't handle non-finite values.
Results may differ from a plain program's by a relative error of at most 0.013.
Values may be sent and summed in bfloat16 or wider, within the bound.
A program may use at most 64 MiB of HBM per device.

v0:
```python
import functools
import math

import jax
import jax.numpy as jnp
import numpy as np
from jax import lax
from jax.experimental import pallas as pl
from jax.experimental.pallas import tpu as pltpu
from jax.sharding import PartitionSpec as P

GROUP_CH = 128


TWO_PI = 2.0 * math.pi
NORM_EPS = 1e-06
HIGHEST = lax.Precision.HIGHEST


def phase_tables(rows, cols, period):
    left = lax.broadcasted_iota(jnp.int32, (rows, cols), 0)
    right = lax.broadcasted_iota(jnp.int32, (rows, cols), 1)
    angles = (left * right % period).astype(jnp.float32) * (TWO_PI / period)
    return (jnp.cos(angles), jnp.sin(angles))


def rotate_by(pattern, cos_table, sin_table, real_part, imag_part):

    def apply(table, data):
        return jnp.einsum(pattern, table, data, precision=HIGHEST)

    return (
        apply(cos_table, real_part) + apply(sin_table, imag_part),
        apply(cos_table, imag_part) - apply(sin_table, real_part),
    )


def twist(real_part, imag_part, cos_table, sin_table):
    return (
        real_part * cos_table + imag_part * sin_table,
        imag_part * cos_table - real_part * sin_table,
    )


def factored_shards(tokens, norm_gain, w_in, w_out):
    seq_count, tok_count, width = tokens.shape
    feat_count = w_in.shape[1]
    row_count = lax.axis_size("row")
    col_count = lax.axis_size("col")
    block_len = tok_count * col_count
    length = block_len * row_count
    sub_feats = feat_count // row_count
    fine_count = tok_count // row_count
    item_count = seq_count * feat_count // col_count
    ortho_scale = 1.0 / math.sqrt(length * GROUP_CH)
    widened = tokens.astype(jnp.float32)
    factor = lax.rsqrt(jnp.mean(widened * widened, -1, keepdims=True) + NORM_EPS)
    normed = (widened * factor * norm_gain.astype(jnp.float32)).astype(jnp.bfloat16)
    mixin = jnp.einsum("std,df->sft", normed, w_in, preferred_element_type=jnp.float32).astype(
        jnp.bfloat16
    )
    row_cos, row_sin = phase_tables(row_count, row_count, row_count)
    chan_cos, chan_sin = phase_tables(GROUP_CH, GROUP_CH, GROUP_CH)
    stacked_shape = (seq_count, sub_feats, row_count, tok_count)
    grouped = mixin.astype(jnp.float32).reshape(
        seq_count, feat_count // GROUP_CH, GROUP_CH, tok_count
    )
    spec_real = jnp.einsum("sgqt,qm->sgmt", grouped, chan_cos, precision=HIGHEST).reshape(
        seq_count, feat_count, tok_count
    )
    spec_imag = -jnp.einsum("sgqt,qm->sgmt", grouped, chan_sin, precision=HIGHEST).reshape(
        seq_count, feat_count, tok_count
    )
    arrived = (
        lax.all_to_all(
            spec_real.astype(jnp.bfloat16), "row", split_axis=1, concat_axis=2, tiled=True
        ).astype(spec_real.dtype),
        lax.all_to_all(
            spec_imag.astype(jnp.bfloat16), "row", split_axis=1, concat_axis=2, tiled=True
        ).astype(spec_imag.dtype),
    )
    stacked_real = arrived[0].reshape(stacked_shape)
    stacked_imag = arrived[1].reshape(stacked_shape)
    real_part, imag_part = rotate_by("ka,sfat->skft", row_cos, row_sin, stacked_real, stacked_imag)
    freq_low = lax.broadcasted_iota(jnp.int32, (row_count, tok_count), 0)
    place = lax.axis_index("col") * tok_count + lax.broadcasted_iota(
        jnp.int32, (row_count, tok_count), 1
    )
    angles = (freq_low * place % length).astype(jnp.float32) * (TWO_PI / length)
    real_part, imag_part = twist(
        real_part, imag_part, jnp.cos(angles)[None, :, None, :], jnp.sin(angles)[None, :, None, :]
    )
    sending = (
        real_part.reshape(item_count, col_count, 1, tok_count),
        imag_part.reshape(item_count, col_count, 1, tok_count),
    )
    col_cos, col_sin = phase_tables(col_count, col_count, col_count)
    mid_cos, mid_sin = phase_tables(col_count, tok_count, block_len)
    tok_cos, tok_sin = phase_tables(tok_count, tok_count, tok_count)
    tok_cos = tok_cos.reshape(row_count, fine_count, tok_count)
    tok_sin = tok_sin.reshape(row_count, fine_count, tok_count)
    span_real, span_imag = rotate_by(
        "uc,qct->qut",
        col_cos,
        col_sin,
        lax.all_to_all(
            sending[0].astype(jnp.bfloat16), "col", split_axis=1, concat_axis=2, tiled=True
        ).astype(jnp.float32)[:, 0],
        lax.all_to_all(
            sending[1].astype(jnp.bfloat16), "col", split_axis=1, concat_axis=2, tiled=True
        ).astype(jnp.float32)[:, 0],
    )
    span_real, span_imag = twist(span_real, span_imag, mid_cos, mid_sin)
    span_real, span_imag = rotate_by("rjt,qut->rjuq", tok_cos, tok_sin, span_real, span_imag)
    owner_shape = (row_count, col_count, fine_count, span_real.shape[-1], 1)
    span_real, span_imag = (span_real.reshape(owner_shape), span_imag.reshape(owner_shape))
    rounded = (span_real * ortho_scale).astype(jnp.bfloat16)
    returned = lax.all_to_all(rounded, "col", split_axis=1, concat_axis=4, tiled=True)
    layout = (row_count, fine_count, seq_count, row_count, sub_feats)
    spectrum = lax.all_to_all(
        returned.reshape(layout), "row", split_axis=0, concat_axis=4, tiled=True
    )
    spectrum = spectrum.reshape(fine_count, seq_count, row_count, feat_count)
    mixed = jnp.einsum("jskf,fd->sjkd", spectrum, w_out, preferred_element_type=jnp.float32).astype(
        jnp.bfloat16
    )
    return mixed.reshape(seq_count, fine_count * row_count, width)


LANES = 128
SUBLANES = 8
MESH = pl.DeviceIdType.MESH
NT = (((1,), (1,)), ((), ()))


def fused_fits(peers, tok_count, feat_count):
    if feat_count % peers or tok_count % peers or GROUP_CH != LANES:
        return False
    slots = feat_count // peers
    return (
        tok_count == LANES
        and slots % (4 * SUBLANES) == 0
        and LANES % slots == 0
        and peers % (LANES // slots) == 0
        and feat_count % GROUP_CH == 0
        and (tok_count // peers) % SUBLANES == 0
    )


def host_tables(peers, tok_count, feat_count):
    length = peers * tok_count
    slots = feat_count // peers
    half = slots // 2
    per_lane = LANES // slots
    stacks = peers // per_lane
    fine = tok_count // peers
    members = GROUP_CH // slots
    chan = np.zeros((GROUP_CH, GROUP_CH))
    chan_at = np.zeros((GROUP_CH,), np.int64)
    q = np.arange(GROUP_CH)
    for m in range(GROUP_CH // 2):
        row = m // half * slots + m % half
        chan[row] = np.cos(2 * np.pi * (q * m % GROUP_CH) / GROUP_CH)
        chan_at[row] = m
        if m:
            chan[row + half] = -np.sin(2 * np.pi * (q * m % GROUP_CH) / GROUP_CH)
            chan_at[row + half] = GROUP_CH - m
        else:
            chan[row + half] = np.cos(np.pi * q)
            chan_at[row + half] = GROUP_CH // 2
    t = np.arange(tok_count)
    b = np.arange(tok_count)[:, None]
    scale = 1.0 / math.sqrt(length * GROUP_CH)
    mid = np.zeros((stacks, tok_count, per_lane, 2, tok_count))
    for g in range(stacks):
        for a in range(per_lane):
            k = peers * b + g * per_lane + a
            angle = 2 * np.pi * (t * k % length) / length
            mid[g, :, a, 0] = np.cos(angle) * scale
            mid[g, :, a, 1] = np.sin(angle) * scale
    mid = mid.reshape(stacks, tok_count, per_lane * 2 * tok_count)
    pick = np.zeros((members, per_lane, slots, per_lane, GROUP_CH))
    for dd in range(members):
        for a in range(per_lane):
            for c in range(slots):
                pick[dd, a, c, a, chan_at[dd * slots + c]] = 1
    pick = pick.reshape(members * LANES, per_lane * GROUP_CH)
    return [jnp.asarray(x, jnp.bfloat16) for x in (chan, mid, pick)]


def short_transform(blocks):
    n = len(blocks)
    even = [blocks[0]] + [blocks[s] + blocks[n - s] for s in range(1, n // 2)] + [blocks[n // 2]]
    odd = [None] + [blocks[s] - blocks[n - s] for s in range(1, n // 2)]

    def combine(terms):
        groups = {}
        for coef, term in terms:
            if abs(coef) < 1e-9:
                continue
            size = round(abs(coef), 9)
            signed = groups.get(size)
            if signed is None:
                groups[size] = term if coef > 0 else -term
            else:
                groups[size] = signed + term if coef > 0 else signed - term
        total = None
        for size, value in groups.items():
            value = value if size == 1.0 else value * size
            total = value if total is None else total + value
        return total

    out = []
    for a in range(n // 2 + 1):
        cos_part = combine(
            [(math.cos(TWO_PI * (s * a % n) / n), even[s]) for s in range(n // 2 + 1)]
        )
        sin_part = combine([(math.sin(TWO_PI * (s * a % n) / n), odd[s]) for s in range(1, n // 2)])
        if sin_part is None:
            sin_part = jnp.zeros_like(cos_part)
        out.append((cos_part, sin_part))
    for a in range(n // 2 + 1, n):
        out.append((out[n - a][0], -out[n - a][1]))
    return out


def fused_kernel(
    shape,
    tokens_hbm,
    gain_hbm,
    w_in_hbm,
    chan_hbm,
    mid_hbm,
    pick_hbm,
    out_ref,
    tokens,
    gain,
    w_in,
    chan,
    mid,
    pick,
    natural,
    first_out,
    first_in,
    blocks,
    second_out,
    second_in,
    load_sem,
    send_a,
    recv_a,
    send_b,
    recv_b,
):
    row_count, col_count = shape
    peers = row_count * col_count
    tok_count, width = tokens.shape
    feat_count = w_in.shape[1]
    slots = feat_count // peers
    half = slots // 2
    per_lane = LANES // slots
    stacks = peers // per_lane
    fine = tok_count // peers
    members = GROUP_CH // slots
    groups = feat_count // GROUP_CH
    me = lax.axis_index("row") * col_count + lax.axis_index("col")

    def peer(step):
        return lax.rem(me + step, peers)

    def device(index):
        return {"row": index // col_count, "col": lax.rem(index, col_count)}

    row, col = lax.axis_index("row"), lax.axis_index("col")
    far_first = []
    for i in range(row_count - 1):
        down = row_count - 1 - i
        down = down - jnp.where(down <= row, 1, 0)
        up = i + jnp.where(i >= row, 1, 0)
        target_row = jnp.where(row * 2 < row_count, down, up)
        far_first += [
            target_row * col_count + lax.rem(col + shift, col_count)
            for shift in [*range(1, col_count), 0]
        ]
    far_first += [row * col_count + lax.rem(col + shift, col_count) for shift in range(1, col_count)]

    chunks = 4
    depth = width // chunks
    loads = [
        pltpu.make_async_copy(tokens_hbm, tokens, load_sem.at[0]),
        pltpu.make_async_copy(gain_hbm, gain, load_sem.at[1]),
    ]
    for i in range(chunks):
        part = pl.ds(i * depth, depth)
        loads.append(pltpu.make_async_copy(w_in_hbm.at[part], w_in.at[part], load_sem.at[2 + i]))
    rest = [(chan_hbm, chan), (mid_hbm, mid), (pick_hbm, pick)]
    for i, (src, dst) in enumerate(rest):
        loads.append(pltpu.make_async_copy(src, dst, load_sem.at[2 + chunks + i]))
    for load in loads[: 3 + chunks]:
        load.start()

    barrier = pltpu.get_barrier_semaphore()
    for step in range(1, peers):
        pl.semaphore_signal(barrier, inc=1, device_id=device(peer(step)), device_id_type=MESH)

    loads[0].wait()
    loads[1].wait()
    widened = tokens[...].astype(jnp.float32)
    factor = lax.rsqrt(jnp.mean(widened * widened, -1, keepdims=True) + NORM_EPS)
    normed = (widened * factor * gain[...].astype(jnp.float32).reshape(1, width)).astype(jnp.bfloat16)
    mixin = None
    for i in range(chunks):
        loads[2 + i].wait()
        term = jnp.dot(
            normed[:, i * depth : (i + 1) * depth],
            w_in[i * depth : (i + 1) * depth, :],
            preferred_element_type=jnp.float32,
        )
        mixin = term if mixin is None else mixin + term
    mixin = mixin.astype(jnp.bfloat16)
    for load in loads[3 + chunks :]:
        load.start()
    loads[2 + chunks].wait()
    for g in range(groups):
        spec = lax.dot_general(
            chan[...],
            mixin[:, g * GROUP_CH : (g + 1) * GROUP_CH],
            NT,
            preferred_element_type=jnp.float32,
        ).astype(jnp.bfloat16)
        for dd in range(members):
            first_out[g * members + dd] = spec[dd * slots : (dd + 1) * slots]
    pl.semaphore_wait(barrier, peers - 1)
    copies = []
    for step, target in enumerate(far_first):
        copy = pltpu.make_async_remote_copy(
            src_ref=first_out.at[target],
            dst_ref=first_in.at[me],
            send_sem=send_a.at[step],
            recv_sem=recv_a.at[me],
            device_id=device(target),
            device_id_type=MESH,
        )
        copy.start()
        copies.append(copy)
    first_in[me] = first_out[me]
    blocks[...] = jnp.zeros_like(blocks)
    for load in loads[3 + chunks :]:
        load.wait()
    for step in range(1, peers):
        source = peer(step)
        pltpu.make_async_copy(first_in.at[source], first_in.at[source], recv_a.at[source]).wait()

    arrived = [first_in[s].astype(jnp.float32) for s in range(peers)]
    place = lax.broadcasted_iota(jnp.int32, (half, tok_count), 0) + me * half
    paired = lax.rem(place, GROUP_CH // 2) != 0
    spectra = short_transform(arrived)
    for a, (cos_part, sin_part) in enumerate(spectra):
        a_cos, b_cos = cos_part[:half], cos_part[half:]
        a_sin, b_sin = sin_part[:half], sin_part[half:]
        top_cos = jnp.where(paired, a_cos + b_sin, a_cos)
        top_sin = jnp.where(paired, b_cos - a_sin, -a_sin)
        low_cos = jnp.where(paired, a_cos - b_sin, b_cos)
        low_sin = jnp.where(paired, -a_sin - b_cos, -b_sin)
        at = a % per_lane
        left = at * 2 * tok_count
        blocks[a // per_lane, at * slots : at * slots + half, left : left + tok_count] = (
            top_cos.astype(jnp.bfloat16)
        )
        blocks[
            a // per_lane, at * slots : at * slots + half, left + tok_count : left + 2 * tok_count
        ] = top_sin.astype(jnp.bfloat16)
        blocks[a // per_lane, at * slots + half : (at + 1) * slots, left : left + tok_count] = (
            low_cos.astype(jnp.bfloat16)
        )
        blocks[
            a // per_lane,
            at * slots + half : (at + 1) * slots,
            left + tok_count : left + 2 * tok_count,
        ] = low_sin.astype(jnp.bfloat16)
    found = []
    for g in range(stacks):
        value = lax.dot_general(mid[g], blocks[g], NT, preferred_element_type=jnp.float32)
        found.append(value.reshape(peers, fine, LANES))
    second_out[...] = jnp.concatenate(found, axis=1).astype(jnp.bfloat16)

    def landing(index):
        lanes = pl.ds(pl.multiple_of(lax.rem(index, members) * LANES, LANES), LANES)
        return second_in.at[index // members, :, lanes]

    returns = []
    for step, target in enumerate(far_first):
        copy = pltpu.make_async_remote_copy(
            src_ref=second_out.at[target],
            dst_ref=landing(me),
            send_sem=send_b.at[step],
            recv_sem=recv_b.at[me],
            device_id=device(target),
            device_id_type=MESH,
        )
        copy.start()
        returns.append(copy)
    landing(me)[...] = second_out[me]
    for copy in copies:
        copy.wait_send()
    for step in range(1, peers):
        source = peer(step)
        pltpu.make_async_copy(landing(source), landing(source), recv_b.at[source]).wait()
    flat = second_in[...].reshape(groups * stacks * fine, members * LANES)
    picked = jnp.dot(flat, pick[...], preferred_element_type=jnp.float32)
    for group in range(groups):
        for g in range(stacks):
            top = (group * stacks + g) * fine
            for a in range(per_lane):
                natural[group, pl.ds(g * per_lane + a, fine, stride=peers), :] = picked[top : top + fine, a * GROUP_CH : (a + 1) * GROUP_CH]
        out_ref[:, group * GROUP_CH : (group + 1) * GROUP_CH] = natural[group].astype(
            out_ref.dtype
        )
    for copy in returns:
        copy.wait_send()


def project_kernel(chunks, spectrum, w_out, out_hbm, staged, sems):
    size = w_out.shape[1] // chunks
    copies = []
    for i in range(chunks):
        lanes = slice(i * size, (i + 1) * size)
        staged[:, lanes] = jnp.dot(
            spectrum[...], w_out[:, lanes], preferred_element_type=jnp.float32
        ).astype(staged.dtype)
        span = pl.ds(i * size, size)
        copy = pltpu.make_async_copy(staged.at[:, span], out_hbm.at[:, span], sems.at[i])
        copy.start()
        copies.append(copy)
    for copy in copies:
        copy.wait()


def fused_shards(tokens, norm_gain, w_in, w_out):
    seq_count, tok_count, width = tokens.shape
    feat_count = w_in.shape[1]
    shape = (lax.axis_size("row"), lax.axis_size("col"))
    peers = shape[0] * shape[1]
    slots = feat_count // peers
    per_lane = LANES // slots
    stacks = peers // per_lane
    fine = tok_count // peers
    members = GROUP_CH // slots
    tables = host_tables(peers, tok_count, feat_count)
    operands = [tokens.reshape(tok_count, width), norm_gain, w_in, *tables]
    held = [pltpu.VMEM(x.shape, x.dtype) for x in operands]
    spectrum = pl.pallas_call(
        functools.partial(fused_kernel, shape),
        out_shape=pltpu.VMEM((tok_count, feat_count), jnp.bfloat16),
        in_specs=[pl.BlockSpec(memory_space=pltpu.HBM)] * len(operands),
        out_specs=pl.BlockSpec(memory_space=pltpu.VMEM),
        scratch_shapes=held
        + [
            pltpu.VMEM((feat_count // GROUP_CH, tok_count, GROUP_CH), jnp.float32),
            pltpu.VMEM((peers, slots, tok_count), jnp.bfloat16),
            pltpu.VMEM((peers, slots, tok_count), jnp.bfloat16),
            pltpu.VMEM((stacks, LANES, per_lane * 2 * tok_count), jnp.bfloat16),
            pltpu.VMEM((peers, stacks * fine, LANES), jnp.bfloat16),
            pltpu.VMEM((peers // members, stacks * fine, members * LANES), jnp.bfloat16),
            pltpu.SemaphoreType.DMA((16,)),
            pltpu.SemaphoreType.DMA((peers,)),
            pltpu.SemaphoreType.DMA((peers,)),
            pltpu.SemaphoreType.DMA((peers,)),
            pltpu.SemaphoreType.DMA((peers,)),
        ],
        compiler_params=pltpu.CompilerParams(
            collective_id=0, has_side_effects=True, vmem_limit_bytes=64_600_000
        ),
    )(*operands)
    chunks = max(1, width // 512)
    mixed = pl.pallas_call(
        functools.partial(project_kernel, chunks),
        out_shape=jax.ShapeDtypeStruct((tok_count, width), jnp.bfloat16),
        in_specs=[pl.BlockSpec(memory_space=pltpu.VMEM)] * 2,
        out_specs=pl.BlockSpec(memory_space=pltpu.HBM),
        scratch_shapes=[
            pltpu.VMEM((tok_count, width), jnp.bfloat16),
            pltpu.SemaphoreType.DMA((chunks,)),
        ],
        compiler_params=pltpu.CompilerParams(vmem_limit_bytes=8 * 1024 * 1024),
    )(spectrum, w_out)
    return mixed.reshape(seq_count, tok_count, width)


def shards(tokens, norm_gain, w_in, w_out):
    peers = lax.axis_size("row") * lax.axis_size("col")
    seq_count, tok_count, _ = tokens.shape
    if seq_count == 1 and fused_fits(peers, tok_count, w_in.shape[1]):
        return fused_shards(tokens, norm_gain, w_in, w_out)
    return factored_shards(tokens, norm_gain, w_in, w_out)


def solution(mesh):
    return jax.shard_map(
        shards,
        mesh=mesh,
        in_specs=(P("grp", ("row", "col"), None), P(), P(), P()),
        out_specs=P("grp", ("row", "col"), None),
        check_vma=False,
    )
```

profile of v0, /device:TPU:0, one launch (start us, length us, event | category | flops | bytes accessed | tf_op | source)
XLA Modules:
  0.0 18.2 jit_solution(2852789495797584162)
XLA Ops:
  0.0 0.0 copy-start
  0.0 17.0 %shard_map.73.spectrum = bf16[128,512]{1,0:T(8,128)(2,1)S(1)} custom-call(bf16[128,2048]{1,0:T(8,128)(2,1)} %bitcast.2, bf16[2048]{0:T(1024)(128)(2,1)} %gain_hbm.1, bf16[2048,512]{1,0:T(8,128)(2,1)} %w_in_hbm.1, bf16[128,128]{1,0:T(8,128)(2,1)} %constant.6.clone.chan_hbm, bf16[4,128,1024]{2,1,0:T(8,128)(2,1)} %constant.7.clone.mid_hbm, ...), custom_call_target="tpu_custom_call" | custom-call | tf_op jit(solution)/shard_map/pallas_call | solution.py:451
  17.1 0.0 copy-done
  17.1 1.1 %shard_map.74 = bf16[128,2048]{1,0:T(8,128)(2,1)} custom-call(bf16[128,512]{1,0:T(8,128)(2,1)S(1)} %shard_map.73.spectrum, bf16[512,2048]{1,0:T(8,128)(2,1)S(1)} %copy-done), custom_call_target="tpu_custom_call" | custom-call | tf_op jit(solution)/shard_map/pallas_call | solution.py:475
Async XLA Ops:
  0.0 17.1 %copy-start = (bf16[512,2048]{1,0:T(8,128)(2,1)S(1)}, bf16[512,2048]{1,0:T(8,128)(2,1)}, u32[]{:S(2)}) copy-start(bf16[512,2048]{1,0:T(8,128)(2,1)} %w_out.1) | copy-start | bytes 6291460
where the time goes:
time: 18.4 us; the launch traced here: 18.2 us
  Pallas kernels  18.2 us (99%)
    pallas_call x1, Pallas kernels, fused_shards(): pl.pallas_call(functools.partial(fused_kernel, shape), out_shape=pltpu.VM...  17 us
    pallas_call x1, Pallas kernels, fused_shards(): pl.pallas_call(functools.partial(project_kernel, chunks), out_shape=jax.S...  1.15 us

commit v1 on v0

--- a/solution.py
+++ b/solution.py
@@ -129,11 +129,15 @@
 
 LANES = 128
 SUBLANES = 8
+CHUNKS = 2
+PIECES = 4
 MESH = pl.DeviceIdType.MESH
 NT = (((1,), (1,)), ((), ()))
 
 
-def fused_fits(peers, tok_count, feat_count):
+def fused_fits(row_count, peers, tok_count, feat_count):
+    if row_count % (2 * CHUNKS) or feat_count % (GROUP_CH * CHUNKS):
+        return False
     if feat_count % peers or tok_count % peers or GROUP_CH != LANES:
         return False
     slots = feat_count // peers
@@ -226,19 +230,24 @@
 
 def fused_kernel(
     shape,
+    chunks,
     tokens_hbm,
     gain_hbm,
     w_in_hbm,
     chan_hbm,
     mid_hbm,
     pick_hbm,
-    out_ref,
+    w_out_hbm,
+    last_ref,
+    partial_ref,
+    w_last,
     tokens,
     gain,
     w_in,
     chan,
     mid,
     pick,
+    w_first,
     natural,
     first_out,
     first_in,
@@ -262,170 +271,275 @@
     fine = tok_count // peers
     members = GROUP_CH // slots
     groups = feat_count // GROUP_CH
-    me = lax.axis_index("row") * col_count + lax.axis_index("col")
-
-    def peer(step):
-        return lax.rem(me + step, peers)
+    hosts = peers // chunks
+    host_rows = row_count // chunks
+    low_row = (row_count - host_rows) // 2
+    high_row = low_row + host_rows - 1
+    part_groups = groups // chunks
+    part_feats = feat_count // chunks
+    row, col = lax.axis_index("row"), lax.axis_index("col")
+    me = row * col_count + col
+    is_host = (row >= low_row) & (row <= high_row)
+    host = jnp.where(is_host, me - low_row * col_count, 0)
 
     def device(index):
         return {"row": index // col_count, "col": lax.rem(index, col_count)}
 
-    row, col = lax.axis_index("row"), lax.axis_index("col")
-    far_first = []
-    for i in range(row_count - 1):
-        down = row_count - 1 - i
-        down = down - jnp.where(down <= row, 1, 0)
-        up = i + jnp.where(i >= row, 1, 0)
-        target_row = jnp.where(row * 2 < row_count, down, up)
-        far_first += [
-            target_row * col_count + lax.rem(col + shift, col_count)
+    depth = width // PIECES
+    load_tokens = pltpu.make_async_copy(tokens_hbm, tokens, load_sem.at[0])
+    load_gain = pltpu.make_async_copy(gain_hbm, gain, load_sem.at[1])
+    load_chan = pltpu.make_async_copy(chan_hbm, chan, load_sem.at[2])
+    load_mid = pltpu.make_async_copy(mid_hbm, mid, load_sem.at[3])
+    load_pick = pltpu.make_async_copy(pick_hbm, pick, load_sem.at[4])
+    first_feats = feat_count - part_feats
+    load_first = pltpu.make_async_copy(
+        w_out_hbm.at[pl.ds(0, first_feats)], w_first, load_sem.at[5]
+    )
+    load_last = pltpu.make_async_copy(
+        w_out_hbm.at[pl.ds(first_feats, part_feats)], w_last, load_sem.at[6]
+    )
+    load_w = []
+    for c in range(chunks):
+        for i in range(PIECES):
+            at = (pl.ds(i * depth, depth), pl.ds(c * part_feats, part_feats))
+            load_w.append(
+                pltpu.make_async_copy(
+                    w_in_hbm.at[at], w_in.at[at], load_sem.at[7 + c * PIECES + i]
+                )
+            )
+    load_tokens.start()
+    load_gain.start()
+    for load in load_w[:PIECES]:
+        load.start()
+    load_chan.start()
+    for load in load_w[PIECES:]:
+        load.start()
+
+    barrier = pltpu.get_barrier_semaphore()
+
+    @pl.when(is_host)
+    def _():
+        for step in range(1, peers):
+            target = lax.rem(me + step, peers)
+            pl.semaphore_signal(barrier, inc=1, device_id=device(target), device_id_type=MESH)
+
+    host_order = []
+    for i in range(host_rows):
+        target_row = jnp.where(row * 2 < row_count, high_row - i, low_row + i)
+        host_order += [
+            (target_row * col_count + lax.rem(col + shift, col_count), shift == 0)
             for shift in [*range(1, col_count), 0]
         ]
-    far_first += [row * col_count + lax.rem(col + shift, col_count) for shift in range(1, col_count)]
-
-    chunks = 4
-    depth = width // chunks
-    loads = [
-        pltpu.make_async_copy(tokens_hbm, tokens, load_sem.at[0]),
-        pltpu.make_async_copy(gain_hbm, gain, load_sem.at[1]),
-    ]
-    for i in range(chunks):
-        part = pl.ds(i * depth, depth)
-        loads.append(pltpu.make_async_copy(w_in_hbm.at[part], w_in.at[part], load_sem.at[2 + i]))
-    rest = [(chan_hbm, chan), (mid_hbm, mid), (pick_hbm, pick)]
-    for i, (src, dst) in enumerate(rest):
-        loads.append(pltpu.make_async_copy(src, dst, load_sem.at[2 + chunks + i]))
-    for load in loads[: 3 + chunks]:
-        load.start()
-
-    barrier = pltpu.get_barrier_semaphore()
-    for step in range(1, peers):
-        pl.semaphore_signal(barrier, inc=1, device_id=device(peer(step)), device_id_type=MESH)
-
-    loads[0].wait()
-    loads[1].wait()
-    widened = tokens[...].astype(jnp.float32)
-    factor = lax.rsqrt(jnp.mean(widened * widened, -1, keepdims=True) + NORM_EPS)
-    normed = (widened * factor * gain[...].astype(jnp.float32).reshape(1, width)).astype(jnp.bfloat16)
-    mixin = None
-    for i in range(chunks):
-        loads[2 + i].wait()
-        term = jnp.dot(
-            normed[:, i * depth : (i + 1) * depth],
-            w_in[i * depth : (i + 1) * depth, :],
-            preferred_element_type=jnp.float32,
-        )
-        mixin = term if mixin is None else mixin + term
-    mixin = mixin.astype(jnp.bfloat16)
-    for load in loads[3 + chunks :]:
-        load.start()
-    loads[2 + chunks].wait()
-    for g in range(groups):
-        spec = lax.dot_general(
-            chan[...],
-            mixin[:, g * GROUP_CH : (g + 1) * GROUP_CH],
-            NT,
-            preferred_element_type=jnp.float32,
-        ).astype(jnp.bfloat16)
-        for dd in range(members):
-            first_out[g * members + dd] = spec[dd * slots : (dd + 1) * slots]
-    pl.semaphore_wait(barrier, peers - 1)
-    copies = []
-    for step, target in enumerate(far_first):
-        copy = pltpu.make_async_remote_copy(
-            src_ref=first_out.at[target],
-            dst_ref=first_in.at[me],
-            send_sem=send_a.at[step],
-            recv_sem=recv_a.at[me],
+
+    def first_copy(c, target):
+        spot = c * hosts + target - low_row * col_count
+        return pltpu.make_async_remote_copy(
+            src_ref=first_out.at[spot],
+            dst_ref=first_in.at[c, me],
+            send_sem=send_a.at[spot],
+            recv_sem=recv_a.at[c, me],
             device_id=device(target),
             device_id_type=MESH,
         )
-        copy.start()
-        copies.append(copy)
-    first_in[me] = first_out[me]
-    blocks[...] = jnp.zeros_like(blocks)
-    for load in loads[3 + chunks :]:
-        load.wait()
-    for step in range(1, peers):
-        source = peer(step)
-        pltpu.make_async_copy(first_in.at[source], first_in.at[source], recv_a.at[source]).wait()
-
-    arrived = [first_in[s].astype(jnp.float32) for s in range(peers)]
-    place = lax.broadcasted_iota(jnp.int32, (half, tok_count), 0) + me * half
-    paired = lax.rem(place, GROUP_CH // 2) != 0
-    spectra = short_transform(arrived)
-    for a, (cos_part, sin_part) in enumerate(spectra):
-        a_cos, b_cos = cos_part[:half], cos_part[half:]
-        a_sin, b_sin = sin_part[:half], sin_part[half:]
-        top_cos = jnp.where(paired, a_cos + b_sin, a_cos)
-        top_sin = jnp.where(paired, b_cos - a_sin, -a_sin)
-        low_cos = jnp.where(paired, a_cos - b_sin, b_cos)
-        low_sin = jnp.where(paired, -a_sin - b_cos, -b_sin)
-        at = a % per_lane
-        left = at * 2 * tok_count
-        blocks[a // per_lane, at * slots : at * slots + half, left : left + tok_count] = (
-            top_cos.astype(jnp.bfloat16)
-        )
-        blocks[
-            a // per_lane, at * slots : at * slots + half, left + tok_count : left + 2 * tok_count
-        ] = top_sin.astype(jnp.bfloat16)
-        blocks[a // per_lane, at * slots + half : (at + 1) * slots, left : left + tok_count] = (
-            low_cos.astype(jnp.bfloat16)
-        )
-        blocks[
-            a // per_lane,
-            at * slots + half : (at + 1) * slots,
-            left + tok_count : left + 2 * tok_count,
-        ] = low_sin.astype(jnp.bfloat16)
-    found = []
-    for g in range(stacks):
-        value = lax.dot_general(mid[g], blocks[g], NT, preferred_element_type=jnp.float32)
-        found.append(value.reshape(peers, fine, LANES))
-    second_out[...] = jnp.concatenate(found, axis=1).astype(jnp.bfloat16)
-
-    def landing(index):
-        lanes = pl.ds(pl.multiple_of(lax.rem(index, members) * LANES, LANES), LANES)
-        return second_in.at[index // members, :, lanes]
-
-    returns = []
-    for step, target in enumerate(far_first):
-        copy = pltpu.make_async_remote_copy(
-            src_ref=second_out.at[target],
-            dst_ref=landing(me),
-            send_sem=send_b.at[step],
-            recv_sem=recv_b.at[me],
+
+    def each_host(c, act):
+        for target, may_be_me in host_order:
+            if may_be_me:
+
+                @pl.when(target != me)
+                def _():
+                    act(first_copy(c, target))
+            else:
+                act(first_copy(c, target))
+
+    load_tokens.wait()
+    load_gain.wait()
+    scaled = tokens[...] * gain[...].reshape(1, width)
+    widened = tokens[...].astype(jnp.float32)
+    factor = lax.rsqrt(jnp.mean(widened * widened, -1, keepdims=True) + NORM_EPS)
+    for c in range(chunks):
+        mixin = None
+        for i in range(PIECES):
+            load_w[c * PIECES + i].wait()
+            term = jnp.dot(
+                scaled[:, i * depth : (i + 1) * depth],
+                w_in[i * depth : (i + 1) * depth, c * part_feats : (c + 1) * part_feats],
+                preferred_element_type=jnp.float32,
+            )
+            mixin = term if mixin is None else mixin + term
+        mixin = (mixin * factor).astype(jnp.bfloat16)
+        if c == 0:
+            load_chan.wait()
+        if c == chunks - 1:
+
+            @pl.when(is_host)
+            def _():
+                load_mid.start()
+
+            load_pick.start()
+            load_first.start()
+            load_last.start()
+        for g in range(part_groups):
+            spec = lax.dot_general(
+                chan[...],
+                mixin[:, g * GROUP_CH : (g + 1) * GROUP_CH],
+                NT,
+                preferred_element_type=jnp.float32,
+            ).astype(jnp.bfloat16)
+            for dd in range(members):
+                spot = (c * part_groups + g) * members + dd
+                first_out[spot] = spec[dd * slots : (dd + 1) * slots]
+        if c == 0:
+
+            @pl.when(is_host)
+            def _():
+                pl.semaphore_wait(barrier, hosts - 1)
+
+            @pl.when(jnp.logical_not(is_host))
+            def _():
+                pl.semaphore_wait(barrier, hosts)
+
+        each_host(c, lambda copy: copy.start())
+
+    def landing(spot):
+        lanes = pl.ds(pl.multiple_of(lax.rem(spot, members) * LANES, LANES), LANES)
+        return second_in.at[spot // members, :, lanes]
+
+    def second_copy(c, target):
+        spot = c * hosts + host
+        return pltpu.make_async_remote_copy(
+            src_ref=second_out.at[c, target],
+            dst_ref=landing(spot),
+            send_sem=send_b.at[c, target],
+            recv_sem=recv_b.at[spot],
             device_id=device(target),
             device_id_type=MESH,
         )
-        copy.start()
-        returns.append(copy)
-    landing(me)[...] = second_out[me]
-    for copy in copies:
-        copy.wait_send()
-    for step in range(1, peers):
-        source = peer(step)
-        pltpu.make_async_copy(landing(source), landing(source), recv_b.at[source]).wait()
-    flat = second_in[...].reshape(groups * stacks * fine, members * LANES)
-    picked = jnp.dot(flat, pick[...], preferred_element_type=jnp.float32)
-    for group in range(groups):
-        for g in range(stacks):
-            top = (group * stacks + g) * fine
-            for a in range(per_lane):
-                natural[group, pl.ds(g * per_lane + a, fine, stride=peers), :] = picked[top : top + fine, a * GROUP_CH : (a + 1) * GROUP_CH]
-        out_ref[:, group * GROUP_CH : (group + 1) * GROUP_CH] = natural[group].astype(
-            out_ref.dtype
+
+    @pl.when(is_host)
+    def _():
+        blocks[...] = jnp.zeros_like(blocks)
+        for c in range(chunks):
+            first_in[c, me] = first_out[c * hosts + host]
+        load_mid.wait()
+        for c in range(chunks):
+            spot = c * hosts + host
+            for step in range(1, peers):
+                source = lax.rem(me + step, peers)
+                pltpu.make_async_copy(
+                    first_in.at[c, source], first_in.at[c, source], recv_a.at[c, source]
+                ).wait()
+            arrived = [first_in[c, s].astype(jnp.float32) for s in range(peers)]
+            place = lax.broadcasted_iota(jnp.int32, (half, tok_count), 0) + spot * half
+            paired = lax.rem(place, GROUP_CH // 2) != 0
+            spectra = short_transform(arrived)
+            for a, (cos_part, sin_part) in enumerate(spectra):
+                a_cos, b_cos = cos_part[:half], cos_part[half:]
+                a_sin, b_sin = sin_part[:half], sin_part[half:]
+                at = a % per_lane
+                left = at * 2 * tok_count
+                tops = slice(at * slots, at * slots + half)
+                lows = slice(at * slots + half, (at + 1) * slots)
+                cosines = slice(left, left + tok_count)
+                sines = slice(left + tok_count, left + 2 * tok_count)
+                g = a // per_lane
+                blocks[c, g, tops, cosines] = jnp.where(paired, a_cos + b_sin, a_cos).astype(
+                    jnp.bfloat16
+                )
+                blocks[c, g, tops, sines] = jnp.where(paired, b_cos - a_sin, -a_sin).astype(
+                    jnp.bfloat16
+                )
+                blocks[c, g, lows, cosines] = jnp.where(paired, a_cos - b_sin, b_cos).astype(
+                    jnp.bfloat16
+                )
+                blocks[c, g, lows, sines] = jnp.where(paired, -a_sin - b_cos, -b_sin).astype(
+                    jnp.bfloat16
+                )
+            found = []
+            for g in range(stacks):
+                value = lax.dot_general(mid[g], blocks[c, g], NT, preferred_element_type=jnp.float32)
+                found.append(value.reshape(peers, fine, LANES))
+            second_out[c] = jnp.concatenate(found, axis=1).astype(jnp.bfloat16)
+            edge_rows = []
+            for i in range(low_row):
+                edge_rows += [i, row_count - 1 - i]
+            for edge in edge_rows:
+                for target in range(edge * col_count, (edge + 1) * col_count):
+                    second_copy(c, target).start()
+            for i in range(1, host_rows + 1):
+                target_row = low_row + lax.rem(row - low_row + i, host_rows)
+                for shift in range(1 if i == host_rows else 0, col_count):
+                    target = target_row * col_count + lax.rem(col + shift, col_count)
+                    second_copy(c, target).start()
+            landing(spot)[...] = second_out[c, me]
+
+    for c in range(chunks):
+        each_host(c, lambda copy: copy.wait_send())
+
+    load_pick.wait()
+    load_first.wait()
+    for c in range(chunks):
+
+        def arrival(spot):
+            pltpu.make_async_copy(landing(spot), landing(spot), recv_b.at[spot]).wait()
+
+        for step in range(1, hosts):
+            arrival(c * hosts + lax.rem(host + step, hosts))
+
+        @pl.when(jnp.logical_not(is_host))
+        def _():
+            arrival(c * hosts + host)
+
+        flat = second_in[c * part_groups : (c + 1) * part_groups].reshape(
+            part_groups * stacks * fine, members * LANES
         )
-    for copy in returns:
-        copy.wait_send()
-
-
-def project_kernel(chunks, spectrum, w_out, out_hbm, staged, sems):
-    size = w_out.shape[1] // chunks
+        picked = jnp.dot(flat, pick[...], preferred_element_type=jnp.float32)
+        for group in range(part_groups):
+            slab = c * part_groups + group
+            for g in range(stacks):
+                top = (group * stacks + g) * fine
+                for a in range(per_lane):
+                    natural[slab, pl.ds(g * per_lane + a, fine, stride=peers), :] = picked[
+                        top : top + fine, a * GROUP_CH : (a + 1) * GROUP_CH
+                    ]
+        if c < chunks - 1:
+            term = None
+            for group in range(part_groups):
+                slab = c * part_groups + group
+                part = jnp.dot(
+                    natural[slab].astype(jnp.bfloat16),
+                    w_first[slab * GROUP_CH : (slab + 1) * GROUP_CH, :],
+                    preferred_element_type=jnp.float32,
+                )
+                term = part if term is None else term + part
+            if c == 0:
+                partial_ref[...] = term
+            else:
+                partial_ref[...] += term
+        if c == chunks - 2:
+
+            @pl.when(is_host)
+            def _():
+                for each in range(chunks):
+                    for step in range(1, peers):
+                        second_copy(each, lax.rem(me + step, peers)).wait_send()
+
+            load_last.wait()
+        if c == chunks - 1:
+            for group in range(part_groups):
+                last_ref[:, group * GROUP_CH : (group + 1) * GROUP_CH] = natural[
+                    c * part_groups + group
+                ].astype(last_ref.dtype)
+
+
+def project_kernel(chunks, last, partial, w_last, out_hbm, staged, sems):
+    size = w_last.shape[1] // chunks
     copies = []
     for i in range(chunks):
         lanes = slice(i * size, (i + 1) * size)
-        staged[:, lanes] = jnp.dot(
-            spectrum[...], w_out[:, lanes], preferred_element_type=jnp.float32
+        staged[:, lanes] = (
+            partial[:, lanes]
+            + jnp.dot(last[...], w_last[:, lanes], preferred_element_type=jnp.float32)
         ).astype(staged.dtype)
         span = pl.ds(i * size, size)
         copy = pltpu.make_async_copy(staged.at[:, span], out_hbm.at[:, span], sems.at[i])
@@ -445,51 +559,58 @@
     stacks = peers // per_lane
     fine = tok_count // peers
     members = GROUP_CH // slots
+    groups = feat_count // GROUP_CH
+    part_feats = feat_count // CHUNKS
     tables = host_tables(peers, tok_count, feat_count)
     operands = [tokens.reshape(tok_count, width), norm_gain, w_in, *tables]
     held = [pltpu.VMEM(x.shape, x.dtype) for x in operands]
-    spectrum = pl.pallas_call(
-        functools.partial(fused_kernel, shape),
-        out_shape=pltpu.VMEM((tok_count, feat_count), jnp.bfloat16),
-        in_specs=[pl.BlockSpec(memory_space=pltpu.HBM)] * len(operands),
-        out_specs=pl.BlockSpec(memory_space=pltpu.VMEM),
+    last, partial, w_last = pl.pallas_call(
+        functools.partial(fused_kernel, shape, CHUNKS),
+        out_shape=(
+            pltpu.VMEM((tok_count, part_feats), jnp.bfloat16),
+            pltpu.VMEM((tok_count, width), jnp.float32),
+            pltpu.VMEM((part_feats, width), jnp.bfloat16),
+        ),
+        in_specs=[pl.BlockSpec(memory_space=pltpu.HBM)] * (len(operands) + 1),
+        out_specs=(pl.BlockSpec(memory_space=pltpu.VMEM),) * 3,
         scratch_shapes=held
         + [
-            pltpu.VMEM((feat_count // GROUP_CH, tok_count, GROUP_CH), jnp.float32),
+            pltpu.VMEM((feat_count - part_feats, width), jnp.bfloat16),
+            pltpu.VMEM((groups, tok_count, GROUP_CH), jnp.float32),
             pltpu.VMEM((peers, slots, tok_count), jnp.bfloat16),
-            pltpu.VMEM((peers, slots, tok_count), jnp.bfloat16),
-            pltpu.VMEM((stacks, LANES, per_lane * 2 * tok_count), jnp.bfloat16),
-            pltpu.VMEM((peers, stacks * fine, LANES), jnp.bfloat16),
+            pltpu.VMEM((CHUNKS, peers, slots, tok_count), jnp.bfloat16),
+            pltpu.VMEM((CHUNKS, stacks, LANES, per_lane * 2 * tok_count), jnp.bfloat16),
+            pltpu.VMEM((CHUNKS, peers, stacks * fine, LANES), jnp.bfloat16),
             pltpu.VMEM((peers // members, stacks * fine, members * LANES), jnp.bfloat16),
-            pltpu.SemaphoreType.DMA((16,)),
+            pltpu.SemaphoreType.DMA((7 + CHUNKS * PIECES,)),
             pltpu.SemaphoreType.DMA((peers,)),
-            pltpu.SemaphoreType.DMA((peers,)),
-            pltpu.SemaphoreType.DMA((peers,)),
+            pltpu.SemaphoreType.DMA((CHUNKS, peers)),
+            pltpu.SemaphoreType.DMA((CHUNKS, peers)),
             pltpu.SemaphoreType.DMA((peers,)),
         ],
         compiler_params=pltpu.CompilerParams(
-            collective_id=0, has_side_effects=True, vmem_limit_bytes=64_600_000
+            collective_id=0, has_side_effects=True, vmem_limit_bytes=62_000_000
         ),
-    )(*operands)
-    chunks = max(1, width // 512)
+    )(*operands, w_out)
+    pieces = max(1, width // 512)
     mixed = pl.pallas_call(
-        functools.partial(project_kernel, chunks),
+        functools.partial(project_kernel, pieces),
         out_shape=jax.ShapeDtypeStruct((tok_count, width), jnp.bfloat16),
-        in_specs=[pl.BlockSpec(memory_space=pltpu.VMEM)] * 2,
+        in_specs=[pl.BlockSpec(memory_space=pltpu.VMEM)] * 3,
         out_specs=pl.BlockSpec(memory_space=pltpu.HBM),
         scratch_shapes=[
             pltpu.VMEM((tok_count, width), jnp.bfloat16),
-            pltpu.SemaphoreType.DMA((chunks,)),
+            pltpu.SemaphoreType.DMA((pieces,)),
         ],
         compiler_params=pltpu.CompilerParams(vmem_limit_bytes=8 * 1024 * 1024),
-    )(spectrum, w_out)
+    )(last, partial, w_last)
     return mixed.reshape(seq_count, tok_count, width)
 
 
 def shards(tokens, norm_gain, w_in, w_out):
     peers = lax.axis_size("row") * lax.axis_size("col")
     seq_count, tok_count, _ = tokens.shape
-    if seq_count == 1 and fused_fits(peers, tok_count, w_in.shape[1]):
+    if seq_count == 1 and fused_fits(lax.axis_size("row"), peers, tok_count, w_in.shape[1]):
         return fused_shards(tokens, norm_gain, w_in, w_out)
     return factored_shards(tokens, norm_gain, w_in, w_out)
 

time: 18.4 us -> 17.2 us (0.935)
  Pallas kernels: 18.2 us -> 17.1 us
    pallas_call x2, Pallas kernels: 18.2 us -> 17.1 us  [the longest x1 16.1 us: fused_shards(): pl.pallas_call(functools.partial(fused_kernel, shape, CHUNKS), out_shape=...]
where the time goes in v1:
time: 17.2 us; the launch traced here: 17.1 us
  Pallas kernels  17.1 us (99%)
    pallas_call x1, Pallas kernels, fused_shards(): pl.pallas_call(functools.partial(fused_kernel, shape, CHUNKS), out_shape=...  16.1 us
    pallas_call x1, Pallas kernels, fused_shards(): pl.pallas_call(functools.partial(project_kernel, pieces), out_shape=jax.S...  1.03 us

profile of v1, /device:TPU:0, one launch (start us, length us, event | category | flops | bytes accessed | tf_op | source)
XLA Modules:
  0.0 17.1 jit_solution(16779402380016939889)
XLA Ops:
  0.0 16.1 %shard_map.73 = (bf16[128,256]{1,0:T(8,128)(2,1)S(1)}, f32[128,2048]{1,0:T(8,128)S(1)}, bf16[256,2048]{1,0:T(8,128)(2,1)S(1)}) custom-call(bf16[128,2048]{1,0:T(8,128)(2,1)} %bitcast.2, bf16[2048]{0:T(1024)(128)(2,1)} %gain_hbm.1, bf16[2048,512]{1,0:T(8,128)(2,1)} %w_in_hbm.1, bf16[128,128]{1,0:T(8,128)(2,1)} %constant.6.clone.chan_hbm, ...), custom_call_target="tpu_custom_call" | custom-call | tf_op jit(solution)/shard_map/pallas_call | solution.py:567
  16.1 1.0 %shard_map.74 = bf16[128,2048]{1,0:T(8,128)(2,1)} custom-call(bf16[128,256]{1,0:T(8,128)(2,1)S(1)} %get-tuple-element.8.last, f32[128,2048]{1,0:T(8,128)S(1)} %get-tuple-element.9.partial, bf16[256,2048]{1,0:T(8,128)(2,1)S(1)} %get-tuple-element.10.w_last), custom_call_target="tpu_custom_call" | custom-call | tf_op jit(solution)/shard_map/pallas_call | solution.py:596

commit v2 on v0

v2 whole, which is shorter than its diff:
```python
import functools
import math

import jax
import jax.numpy as jnp
import numpy as np
from jax import lax
from jax.experimental import pallas as pl
from jax.experimental.pallas import tpu as pltpu
from jax.sharding import PartitionSpec as P

GROUP_CH = 128


TWO_PI = 2.0 * math.pi
NORM_EPS = 1e-06
HIGHEST = lax.Precision.HIGHEST


def phase_tables(rows, cols, period):
    left = lax.broadcasted_iota(jnp.int32, (rows, cols), 0)
    right = lax.broadcasted_iota(jnp.int32, (rows, cols), 1)
    angles = (left * right % period).astype(jnp.float32) * (TWO_PI / period)
    return (jnp.cos(angles), jnp.sin(angles))


def rotate_by(pattern, cos_table, sin_table, real_part, imag_part):

    def apply(table, data):
        return jnp.einsum(pattern, table, data, precision=HIGHEST)

    return (
        apply(cos_table, real_part) + apply(sin_table, imag_part),
        apply(cos_table, imag_part) - apply(sin_table, real_part),
    )


def twist(real_part, imag_part, cos_table, sin_table):
    return (
        real_part * cos_table + imag_part * sin_table,
        imag_part * cos_table - real_part * sin_table,
    )


def factored_shards(tokens, norm_gain, w_in, w_out):
    seq_count, tok_count, width = tokens.shape
    feat_count = w_in.shape[1]
    row_count = lax.axis_size("row")
    col_count = lax.axis_size("col")
    block_len = tok_count * col_count
    length = block_len * row_count
    sub_feats = feat_count // row_count
    fine_count = tok_count // row_count
    item_count = seq_count * feat_count // col_count
    ortho_scale = 1.0 / math.sqrt(length * GROUP_CH)
    widened = tokens.astype(jnp.float32)
    factor = lax.rsqrt(jnp.mean(widened * widened, -1, keepdims=True) + NORM_EPS)
    normed = (widened * factor * norm_gain.astype(jnp.float32)).astype(jnp.bfloat16)
    mixin = jnp.einsum("std,df->sft", normed, w_in, preferred_element_type=jnp.float32).astype(
        jnp.bfloat16
    )
    row_cos, row_sin = phase_tables(row_count, row_count, row_count)
    chan_cos, chan_sin = phase_tables(GROUP_CH, GROUP_CH, GROUP_CH)
    stacked_shape = (seq_count, sub_feats, row_count, tok_count)
    grouped = mixin.astype(jnp.float32).reshape(
        seq_count, feat_count // GROUP_CH, GROUP_CH, tok_count
    )
    spec_real = jnp.einsum("sgqt,qm->sgmt", grouped, chan_cos, precision=HIGHEST).reshape(
        seq_count, feat_count, tok_count
    )
    spec_imag = -jnp.einsum("sgqt,qm->sgmt", grouped, chan_sin, precision=HIGHEST).reshape(
        seq_count, feat_count, tok_count
    )
    arrived = (
        lax.all_to_all(
            spec_real.astype(jnp.bfloat16), "row", split_axis=1, concat_axis=2, tiled=True
        ).astype(spec_real.dtype),
        lax.all_to_all(
            spec_imag.astype(jnp.bfloat16), "row", split_axis=1, concat_axis=2, tiled=True
        ).astype(spec_imag.dtype),
    )
    stacked_real = arrived[0].reshape(stacked_shape)
    stacked_imag = arrived[1].reshape(stacked_shape)
    real_part, imag_part = rotate_by("ka,sfat->skft", row_cos, row_sin, stacked_real, stacked_imag)
    freq_low = lax.broadcasted_iota(jnp.int32, (row_count, tok_count), 0)
    place = lax.axis_index("col") * tok_count + lax.broadcasted_iota(
        jnp.int32, (row_count, tok_count), 1
    )
    angles = (freq_low * place % length).astype(jnp.float32) * (TWO_PI / length)
    real_part, imag_part = twist(
        real_part, imag_part, jnp.cos(angles)[None, :, None, :], jnp.sin(angles)[None, :, None, :]
    )
    sending = (
        real_part.reshape(item_count, col_count, 1, tok_count),
        imag_part.reshape(item_count, col_count, 1, tok_count),
    )
    col_cos, col_sin = phase_tables(col_count, col_count, col_count)
    mid_cos, mid_sin = phase_tables(col_count, tok_count, block_len)
    tok_cos, tok_sin = phase_tables(tok_count, tok_count, tok_count)
    tok_cos = tok_cos.reshape(row_count, fine_count, tok_count)
    tok_sin = tok_sin.reshape(row_count, fine_count, tok_count)
    span_real, span_imag = rotate_by(
        "uc,qct->qut",
        col_cos,
        col_sin,
        lax.all_to_all(
            sending[0].astype(jnp.bfloat16), "col", split_axis=1, concat_axis=2, tiled=True
        ).astype(jnp.float32)[:, 0],
        lax.all_to_all(
            sending[1].astype(jnp.bfloat16), "col", split_axis=1, concat_axis=2, tiled=True
        ).astype(jnp.float32)[:, 0],
    )
    span_real, span_imag = twist(span_real, span_imag, mid_cos, mid_sin)
    span_real, span_imag = rotate_by("rjt,qut->rjuq", tok_cos, tok_sin, span_real, span_imag)
    owner_shape = (row_count, col_count, fine_count, span_real.shape[-1], 1)
    span_real, span_imag = (span_real.reshape(owner_shape), span_imag.reshape(owner_shape))
    rounded = (span_real * ortho_scale).astype(jnp.bfloat16)
    returned = lax.all_to_all(rounded, "col", split_axis=1, concat_axis=4, tiled=True)
    layout = (row_count, fine_count, seq_count, row_count, sub_feats)
    spectrum = lax.all_to_all(
        returned.reshape(layout), "row", split_axis=0, concat_axis=4, tiled=True
    )
    spectrum = spectrum.reshape(fine_count, seq_count, row_count, feat_count)
    mixed = jnp.einsum("jskf,fd->sjkd", spectrum, w_out, preferred_element_type=jnp.float32).astype(
        jnp.bfloat16
    )
    return mixed.reshape(seq_count, fine_count * row_count, width)


CHUNKS = 4
LANES = 128
MESH = pl.DeviceIdType.MESH


def host_spots(row_count, col_count):
    rows = (row_count // 2 - 1, row_count // 2)
    return [(row, col) for row in rows for col in range(1, col_count, 2)]


def fused_fits(row_count, col_count, tok_count, feat_count):
    peers = row_count * col_count
    return (
        row_count >= 4
        and peers == 16
        and tok_count == LANES
        and GROUP_CH == LANES
        and feat_count == GROUP_CH * len(host_spots(row_count, col_count))
        and feat_count > GROUP_CH
    )


def row_slots(peers):
    slots = [0, peers // 2]
    for a in range(1, peers // 2):
        slots += [a, peers - a]
    return slots


def host_tables(peers, tok_count):
    length = peers * tok_count
    half = GROUP_CH // 2
    q = np.arange(GROUP_CH)[:, None]
    m = np.arange(half)[None, :]
    chan = np.zeros((GROUP_CH, GROUP_CH))
    chan[:, :half] = np.cos(2 * np.pi * (q * m % GROUP_CH) / GROUP_CH)
    chan[:, half:] = -np.sin(2 * np.pi * (q * m % GROUP_CH) / GROUP_CH)
    chan[:, half] = np.cos(np.pi * q[:, 0])
    t = np.arange(tok_count)[None, :]
    b = np.arange(tok_count)[:, None]
    scale = 1.0 / math.sqrt(length * GROUP_CH)
    mid = np.zeros((peers, tok_count, 2, tok_count))
    for a in range(peers):
        angle = 2 * np.pi * (t * (peers * b + a) % length) / length
        mid[a, :, 0] = np.cos(angle) * scale
        mid[a, :, 1] = -np.sin(angle) * scale * (1 if a <= peers // 2 else -1)
    mid = mid.reshape(peers, tok_count, 2 * tok_count)
    fold = np.zeros((GROUP_CH, GROUP_CH))
    fold[0, 0] = 1
    fold[half, half] = 1
    for a in range(1, half):
        fold[a, a] = 1
        fold[a, GROUP_CH - a] = 1
        fold[half + a, a] = 1
        fold[half + a, GROUP_CH - a] = -1
    return [jnp.asarray(x, jnp.bfloat16) for x in (chan, mid, fold)]


def short_transform(x):
    r = math.sqrt(0.5)
    c1, s1 = math.cos(math.pi / 8), math.sin(math.pi / 8)
    e = [x[s] + x[s + 8] for s in range(8)]
    o = [x[s] - x[s + 8] for s in range(8)]
    p04, n04 = e[0] + e[4], e[0] - e[4]
    p26, n26 = e[2] + e[6], e[2] - e[6]
    p15, n15 = e[1] + e[5], e[1] - e[5]
    p37, n37 = e[3] + e[7], e[3] - e[7]
    low, high = p04 + p26, p15 + p37
    even_cos = (n15 - n37) * r
    even_sin = (n15 + n37) * r
    found = {
        0: (low + high, None),
        8: (low - high, None),
        4: (p04 - p26, p15 - p37),
        2: (n04 + even_cos, even_sin + n26),
        6: (n04 - even_cos, even_sin - n26),
    }
    f1, f2, f3 = o[1] - o[7], (o[2] - o[6]) * r, o[3] - o[5]
    g1, g2, g3 = o[1] + o[7], (o[2] + o[6]) * r, o[3] + o[5]
    up, down = o[0] + f2, o[0] - f2
    one, two = f1 * c1 + f3 * s1, f1 * s1 - f3 * c1
    cosines = {1: up + one, 7: up - one, 3: down + two, 5: down - two}
    plus, minus = g2 + o[4], g2 - o[4]
    three, four = g1 * s1 + g3 * c1, g1 * c1 - g3 * s1
    sines = {1: three + plus, 7: three - plus, 3: four + minus, 5: four - minus}
    for a in (1, 3, 5, 7):
        found[a] = (cosines[a], sines[a])
    return found


def fused_kernel(
    shape,
    tokens_hbm,
    gain_hbm,
    w_in_hbm,
    chan_hbm,
    mid_hbm,
    fold_hbm,
    w_out_hbm,
    last_ref,
    partial_ref,
    w_last,
    tokens,
    gain,
    w_in,
    chan,
    mid,
    fold,
    w_out,
    w_first,
    natural,
    first_out,
    first_in,
    blocks,
    second_out,
    second_in,
    load_sem,
    send_sem,
    recv_a,
    recv_b,
):
    row_count, col_count = shape
    peers = row_count * col_count
    tok_count, width = tokens.shape
    feat_count = w_in.shape[1]
    fine = tok_count // peers
    groups = feat_count // GROUP_CH
    half = GROUP_CH // 2
    spots = host_spots(row_count, col_count)
    hosts = [r * col_count + c for r, c in spots]
    row, col = lax.axis_index("row"), lax.axis_index("col")
    me = row * col_count + col
    is_host = me == hosts[0]
    group = jnp.int32(0)
    for g in range(1, groups):
        is_host = is_host | (me == hosts[g])
        group = group + jnp.where(me == hosts[g], g, 0)

    def device(index):
        return {"row": index // col_count, "col": index % col_count}

    load_tokens = pltpu.make_async_copy(tokens_hbm, tokens, load_sem.at[0])
    load_gain = pltpu.make_async_copy(gain_hbm, gain, load_sem.at[1])
    load_chan = pltpu.make_async_copy(chan_hbm, chan, load_sem.at[2])
    load_mid = pltpu.make_async_copy(mid_hbm, mid, load_sem.at[3])
    load_fold = pltpu.make_async_copy(fold_hbm, fold, load_sem.at[4])
    load_out = pltpu.make_async_copy(w_out_hbm, w_out, load_sem.at[5])
    size = feat_count // CHUNKS
    load_w = []
    for c in range(CHUNKS):
        at = (slice(None), pl.ds(c * size, size))
        load_w.append(pltpu.make_async_copy(w_in_hbm.at[at], w_in.at[at], load_sem.at[6 + c]))
    load_tokens.start()
    load_gain.start()
    load_w[0].start()
    load_chan.start()
    for load in load_w[1:]:
        load.start()

    barrier = pltpu.get_barrier_semaphore()

    @pl.when(is_host)
    def _():
        for step in range(1, peers):
            target = lax.rem(me + step, peers)
            pl.semaphore_signal(
                barrier,
                inc=1,
                device_id={"row": target // col_count, "col": lax.rem(target, col_count)},
                device_id_type=MESH,
            )

    load_tokens.wait()
    load_gain.wait()
    scaled = tokens[...] * gain[...].reshape(1, width)
    widened = tokens[...].astype(jnp.float32)
    factor = lax.rsqrt(jnp.mean(widened * widened, -1, keepdims=True) + NORM_EPS)
    for c in range(CHUNKS):
        load_w[c].wait()
        if c == CHUNKS - 1:
            load_fold.start()

            @pl.when(is_host)
            def _():
                load_mid.start()

            load_out.start()
        mixin = jnp.dot(
            scaled, w_in[:, c * size : (c + 1) * size], preferred_element_type=jnp.float32
        )
        mixin = (mixin * factor).astype(jnp.bfloat16)
        if c == 0:
            load_chan.wait()
        for i in range(size // GROUP_CH):
            g = c * (size // GROUP_CH) + i
            first_out[g] = jnp.dot(
                mixin[:, i * GROUP_CH : (i + 1) * GROUP_CH],
                chan[...],
                preferred_element_type=jnp.float32,
            ).astype(jnp.bfloat16)
            if g == 0:

                @pl.when(is_host)
                def _():
                    pl.semaphore_wait(barrier, groups - 1)

                @pl.when(jnp.logical_not(is_host))
                def _():
                    pl.semaphore_wait(barrier, groups)

            @pl.when(me != hosts[g])
            def _():
                pltpu.make_async_remote_copy(
                    src_ref=first_out.at[g],
                    dst_ref=first_in.at[me],
                    send_sem=send_sem.at[0],
                    recv_sem=recv_a.at[0],
                    device_id=device(hosts[g]),
                    device_id_type=MESH,
                ).start()

            @pl.when(me == hosts[g])
            def _():
                first_in[me] = first_out[g]

    load_fold.wait()
    load_out.wait()
    for g in range(groups):
        span = slice(g * GROUP_CH, (g + 1) * GROUP_CH)
        folded = jnp.dot(fold[...], w_out[span, :], preferred_element_type=jnp.float32)
        if g < groups - 1:
            w_first[span, :] = folded.astype(jnp.bfloat16)
        else:
            w_last[...] = folded.astype(jnp.bfloat16)

    slots = row_slots(peers)

    @pl.when(is_host)
    def _():
        load_mid.wait()
        rest = first_in.at[pl.ds(0, peers - 1)]
        pltpu.make_async_copy(rest, rest, recv_a.at[0]).wait()
        step = 16
        cosine_lane = lax.broadcasted_iota(jnp.int32, (step, LANES), 1) <= half
        for top in range(0, tok_count, step):
            arrived = [first_in[s, top : top + step].astype(jnp.float32) for s in range(peers)]
            for a, (cosine, sine) in short_transform(arrived).items():
                if sine is None:
                    upper = jnp.where(cosine_lane, cosine, 0.0)
                    lower = jnp.where(cosine_lane, 0.0, -cosine)
                else:
                    upper = jnp.where(cosine_lane, cosine, sine)
                    lower = jnp.where(cosine_lane, sine, -cosine)
                blocks[a, top : top + step] = upper.astype(jnp.bfloat16)
                blocks[a, tok_count + top : tok_count + top + step] = lower.astype(jnp.bfloat16)
        for i in range(0, peers, 2):
            pair = [
                jnp.dot(
                    mid[a], blocks[min(a, peers - a)], preferred_element_type=jnp.float32
                ).reshape(peers, fine, LANES)
                for a in slots[i : i + 2]
            ]
            second_out[:, i * fine : (i + 2) * fine, :] = jnp.concatenate(pair, axis=1).astype(
                jnp.bfloat16
            )

        def send(target):
            pltpu.make_async_remote_copy(
                src_ref=second_out.at[target],
                dst_ref=second_in.at[group],
                send_sem=send_sem.at[1],
                recv_sem=recv_b.at[group],
                device_id={"row": target // col_count, "col": lax.rem(target, col_count)},
                device_id_type=MESH,
            ).start()

        low = spots[0][0]
        for i in range(low):
            for edge in (i, row_count - 1 - i):
                for c in range(col_count):
                    send(edge * col_count + c)
        other = low * 2 + 1 - row
        for c in range(col_count):
            send(other * col_count + c)
        for shift in range(1, col_count):
            send(row * col_count + lax.rem(col + shift, col_count))
        second_in[group] = second_out[me]

    @pl.when(is_host)
    def _():
        sent = first_out.at[pl.ds(0, groups - 1)]
        pltpu.make_async_copy(sent, sent, send_sem.at[0]).wait()

    @pl.when(jnp.logical_not(is_host))
    def _():
        pltpu.make_async_copy(first_out, first_out, send_sem.at[0]).wait()

    flipped = jnp.where(lax.broadcasted_iota(jnp.int32, (fine, LANES), 1) > half, -1.0, 1.0)

    def collect(g):
        @pl.when(me != hosts[g])
        def _():
            pltpu.make_async_copy(second_in.at[g], second_in.at[g], recv_b.at[g]).wait()

        for i, a in enumerate(slots):
            part = second_in[g, i * fine : (i + 1) * fine].astype(jnp.float32)
            if a > peers // 2:
                part = part * flipped
            natural[g, pl.ds(a, fine, stride=peers), :] = part
        return natural[g].astype(jnp.bfloat16)

    def project(g, value):
        return jnp.dot(
            value,
            w_first[g * GROUP_CH : (g + 1) * GROUP_CH, :],
            preferred_element_type=jnp.float32,
        )

    for g in range(groups - 1):
        term = project(g, collect(g))
        if g == 0:
            partial_ref[...] = term
        else:
            partial_ref[...] += term

    @pl.when(is_host)
    def _():
        sent = second_out.at[pl.ds(0, peers - 1)]
        pltpu.make_async_copy(sent, sent, send_sem.at[1]).wait()

    last_ref[...] = collect(groups - 1)


def project_kernel(chunks, last, partial, w_last, out_hbm, staged, sem):
    size = w_last.shape[1] // chunks
    for i in range(chunks):
        lanes = slice(i * size, (i + 1) * size)
        staged[:, lanes] = (
            partial[:, lanes]
            + jnp.dot(last[...], w_last[:, lanes], preferred_element_type=jnp.float32)
        ).astype(staged.dtype)
        span = pl.ds(i * size, size)
        pltpu.make_async_copy(staged.at[:, span], out_hbm.at[:, span], sem).start()
    pltpu.make_async_copy(staged, out_hbm, sem).wait()


def fused_shards(tokens, norm_gain, w_in, w_out):
    seq_count, tok_count, width = tokens.shape
    feat_count = w_in.shape[1]
    shape = (lax.axis_size("row"), lax.axis_size("col"))
    peers = shape[0] * shape[1]
    groups = feat_count // GROUP_CH
    tables = host_tables(peers, tok_count)
    operands = [tokens.reshape(tok_count, width), norm_gain, w_in, *tables, w_out]
    held = [pltpu.VMEM(x.shape, x.dtype) for x in operands]
    last, partial, w_last = pl.pallas_call(
        functools.partial(fused_kernel, shape),
        out_shape=(
            pltpu.VMEM((tok_count, GROUP_CH), jnp.bfloat16),
            pltpu.VMEM((tok_count, width), jnp.float32),
            pltpu.VMEM((GROUP_CH, width), jnp.bfloat16),
        ),
        in_specs=[pl.BlockSpec(memory_space=pltpu.HBM)] * len(operands),
        out_specs=(pl.BlockSpec(memory_space=pltpu.VMEM),) * 3,
        scratch_shapes=held
        + [
            pltpu.VMEM((feat_count - GROUP_CH, width), jnp.bfloat16),
            pltpu.VMEM((groups, tok_count, GROUP_CH), jnp.float32),
            pltpu.VMEM((groups, tok_count, GROUP_CH), jnp.bfloat16),
            pltpu.VMEM((peers, tok_count, GROUP_CH), jnp.bfloat16),
            pltpu.VMEM((peers // 2 + 1, 2 * tok_count, GROUP_CH), jnp.bfloat16),
            pltpu.VMEM((peers, tok_count, GROUP_CH), jnp.bfloat16),
            pltpu.VMEM((groups, tok_count, GROUP_CH), jnp.bfloat16),
            pltpu.SemaphoreType.DMA((6 + CHUNKS,)),
            pltpu.SemaphoreType.DMA((2,)),
            pltpu.SemaphoreType.DMA((1,)),
            pltpu.SemaphoreType.DMA((groups,)),
        ],
        compiler_params=pltpu.CompilerParams(
            collective_id=0, has_side_effects=True, vmem_limit_bytes=62_000_000
        ),
    )(*operands)
    pieces = max(1, width // 512)
    mixed = pl.pallas_call(
        functools.partial(project_kernel, pieces),
        out_shape=jax.ShapeDtypeStruct((tok_count, width), jnp.bfloat16),
        in_specs=[pl.BlockSpec(memory_space=pltpu.VMEM)] * 3,
        out_specs=pl.BlockSpec(memory_space=pltpu.HBM),
        scratch_shapes=[pltpu.VMEM((tok_count, width), jnp.bfloat16), pltpu.SemaphoreType.DMA],
        compiler_params=pltpu.CompilerParams(vmem_limit_bytes=8 * 1024 * 1024),
    )(last, partial, w_last)
    return mixed.reshape(seq_count, tok_count, width)


def shards(tokens, norm_gain, w_in, w_out):
    seq_count, tok_count, _ = tokens.shape
    shape = (lax.axis_size("row"), lax.axis_size("col"))
    if seq_count == 1 and fused_fits(*shape, tok_count, w_in.shape[1]):
        return fused_shards(tokens, norm_gain, w_in, w_out)
    return factored_shards(tokens, norm_gain, w_in, w_out)


def solution(mesh):
    return jax.shard_map(
        shards,
        mesh=mesh,
        in_specs=(P("grp", ("row", "col"), None), P(), P(), P()),
        out_specs=P("grp", ("row", "col"), None),
        check_vma=False,
    )
```

time: 18.4 us -> 15.4 us (0.84)
  Pallas kernels: 18.2 us -> 15.2 us
    pallas_call x2, Pallas kernels: 18.2 us -> 15.2 us  [the longest x1 14.3 us: fused_shards(): pl.pallas_call(functools.partial(fused_kernel, shape), out_shape=(pltpu.V...]
where the time goes in v2:
time: 15.4 us; the launch traced here: 15.2 us
  Pallas kernels  15.2 us (99%)
    pallas_call x1, Pallas kernels, fused_shards(): pl.pallas_call(functools.partial(fused_kernel, shape), out_shape=(pltpu.V...  14.3 us
    pallas_call x1, Pallas kernels, fused_shards(): pl.pallas_call(functools.partial(project_kernel, pieces), out_shape=jax.S...  0.98 us

profile of v2, /device:TPU:0, one launch (start us, length us, event | category | flops | bytes accessed | tf_op | source)
XLA Modules:
  0.0 15.2 jit_solution(7815101168189684762)
XLA Ops:
  0.0 14.3 %shard_map.73 = (bf16[128,128]{1,0:T(8,128)(2,1)S(1)}, f32[128,2048]{1,0:T(8,128)S(1)}, bf16[128,2048]{1,0:T(8,128)(2,1)S(1)}) custom-call(bf16[128,2048]{1,0:T(8,128)(2,1)} %bitcast.2, bf16[2048]{0:T(1024)(128)(2,1)} %gain_hbm.1, bf16[2048,512]{1,0:T(8,128)(2,1)} %w_in_hbm.1, bf16[128,128]{1,0:T(8,128)(2,1)} %constant.6.clone.chan_hbm, ...), custom_call_target="tpu_custom_call" | custom-call | tf_op jit(solution)/shard_map/pallas_call | solution.py:485
  14.3 1.0 %shard_map.74 = bf16[128,2048]{1,0:T(8,128)(2,1)} custom-call(bf16[128,128]{1,0:T(8,128)(2,1)S(1)} %get-tuple-element.8.last, f32[128,2048]{1,0:T(8,128)S(1)} %get-tuple-element.9.partial, bf16[128,2048]{1,0:T(8,128)(2,1)S(1)} %get-tuple-element.10.w_last), custom_call_target="tpu_custom_call" | custom-call | tf_op jit(solution)/shard_map/pallas_call | solution.py:513

commit v3 on v2

--- a/solution.py
+++ b/solution.py
@@ -128,32 +128,29 @@
 
 
 CHUNKS = 4
+LATE = 2
 LANES = 128
 MESH = pl.DeviceIdType.MESH
 
 
-def host_spots(row_count, col_count):
-    rows = (row_count // 2 - 1, row_count // 2)
-    return [(row, col) for row in rows for col in range(1, col_count, 2)]
+def host_spots(row_count):
+    low, high = row_count // 2 - 1, row_count // 2
+    return [(low, 1), (low, 3), (high, 3), (high, 1)]
 
 
 def fused_fits(row_count, col_count, tok_count, feat_count):
-    peers = row_count * col_count
     return (
-        row_count >= 4
-        and peers == 16
+        row_count == 4
+        and col_count == 4
         and tok_count == LANES
         and GROUP_CH == LANES
-        and feat_count == GROUP_CH * len(host_spots(row_count, col_count))
-        and feat_count > GROUP_CH
+        and feat_count == GROUP_CH * 4
     )
 
 
 def row_slots(peers):
-    slots = [0, peers // 2]
-    for a in range(1, peers // 2):
-        slots += [a, peers - a]
-    return slots
+    pairs = [(0, peers // 2)] + [(a, peers - a) for a in range(1, peers // 2)]
+    return [a for parity in (0, 1) for pair in pairs if pair[0] % 2 == parity for a in pair]
 
 
 def host_tables(peers, tok_count):
@@ -173,7 +170,7 @@
         angle = 2 * np.pi * (t * (peers * b + a) % length) / length
         mid[a, :, 0] = np.cos(angle) * scale
         mid[a, :, 1] = -np.sin(angle) * scale * (1 if a <= peers // 2 else -1)
-    mid = mid.reshape(peers, tok_count, 2 * tok_count)
+    mid = mid.reshape(peers, tok_count, 2 * tok_count)[row_slots(peers)]
     fold = np.zeros((GROUP_CH, GROUP_CH))
     fold[0, 0] = 1
     fold[half, half] = 1
@@ -182,14 +179,12 @@
         fold[a, GROUP_CH - a] = 1
         fold[half + a, a] = 1
         fold[half + a, GROUP_CH - a] = -1
-    return [jnp.asarray(x, jnp.bfloat16) for x in (chan, mid, fold)]
-
-
-def short_transform(x):
+    return [jnp.asarray(x, jnp.bfloat16) for x in (np.stack([chan, fold]), mid)]
+
+
+def even_transform(x):
     r = math.sqrt(0.5)
-    c1, s1 = math.cos(math.pi / 8), math.sin(math.pi / 8)
-    e = [x[s] + x[s + 8] for s in range(8)]
-    o = [x[s] - x[s + 8] for s in range(8)]
+    e = [(x[s] + x[s + 8]).astype(jnp.float32) for s in range(8)]
     p04, n04 = e[0] + e[4], e[0] - e[4]
     p26, n26 = e[2] + e[6], e[2] - e[6]
     p15, n15 = e[1] + e[5], e[1] - e[5]
@@ -197,24 +192,31 @@
     low, high = p04 + p26, p15 + p37
     even_cos = (n15 - n37) * r
     even_sin = (n15 + n37) * r
-    found = {
+    return {
         0: (low + high, None),
         8: (low - high, None),
         4: (p04 - p26, p15 - p37),
         2: (n04 + even_cos, even_sin + n26),
         6: (n04 - even_cos, even_sin - n26),
     }
+
+
+def odd_transform(x):
+    r = math.sqrt(0.5)
+    c1, s1 = math.cos(math.pi / 8), math.sin(math.pi / 8)
+    o = [(x[s] - x[s + 8]).astype(jnp.float32) for s in range(8)]
     f1, f2, f3 = o[1] - o[7], (o[2] - o[6]) * r, o[3] - o[5]
     g1, g2, g3 = o[1] + o[7], (o[2] + o[6]) * r, o[3] + o[5]
     up, down = o[0] + f2, o[0] - f2
     one, two = f1 * c1 + f3 * s1, f1 * s1 - f3 * c1
-    cosines = {1: up + one, 7: up - one, 3: down + two, 5: down - two}
     plus, minus = g2 + o[4], g2 - o[4]
     three, four = g1 * s1 + g3 * c1, g1 * c1 - g3 * s1
-    sines = {1: three + plus, 7: three - plus, 3: four + minus, 5: four - minus}
-    for a in (1, 3, 5, 7):
-        found[a] = (cosines[a], sines[a])
-    return found
+    return {
+        1: (up + one, three + plus),
+        7: (up - one, three - plus),
+        3: (down + two, four + minus),
+        5: (down - two, four - minus),
+    }
 
 
 def fused_kernel(
@@ -222,9 +224,8 @@
     tokens_hbm,
     gain_hbm,
     w_in_hbm,
-    chan_hbm,
+    small_hbm,
     mid_hbm,
-    fold_hbm,
     w_out_hbm,
     last_ref,
     partial_ref,
@@ -232,9 +233,8 @@
     tokens,
     gain,
     w_in,
-    chan,
+    small,
     mid,
-    fold,
     w_out,
     w_first,
     natural,
@@ -255,34 +255,30 @@
     fine = tok_count // peers
     groups = feat_count // GROUP_CH
     half = GROUP_CH // 2
-    spots = host_spots(row_count, col_count)
-    hosts = [r * col_count + c for r, c in spots]
+    hosts = [r * col_count + c for r, c in host_spots(row_count)]
     row, col = lax.axis_index("row"), lax.axis_index("col")
     me = row * col_count + col
     is_host = me == hosts[0]
-    group = jnp.int32(0)
-    for g in range(1, groups):
-        is_host = is_host | (me == hosts[g])
-        group = group + jnp.where(me == hosts[g], g, 0)
+    for spot in hosts[1:]:
+        is_host = is_host | (me == spot)
 
     def device(index):
         return {"row": index // col_count, "col": index % col_count}
 
     load_tokens = pltpu.make_async_copy(tokens_hbm, tokens, load_sem.at[0])
     load_gain = pltpu.make_async_copy(gain_hbm, gain, load_sem.at[1])
-    load_chan = pltpu.make_async_copy(chan_hbm, chan, load_sem.at[2])
+    load_small = pltpu.make_async_copy(small_hbm, small, load_sem.at[2])
     load_mid = pltpu.make_async_copy(mid_hbm, mid, load_sem.at[3])
-    load_fold = pltpu.make_async_copy(fold_hbm, fold, load_sem.at[4])
-    load_out = pltpu.make_async_copy(w_out_hbm, w_out, load_sem.at[5])
+    load_out = pltpu.make_async_copy(w_out_hbm, w_out, load_sem.at[4])
     size = feat_count // CHUNKS
     load_w = []
     for c in range(CHUNKS):
         at = (slice(None), pl.ds(c * size, size))
-        load_w.append(pltpu.make_async_copy(w_in_hbm.at[at], w_in.at[at], load_sem.at[6 + c]))
+        load_w.append(pltpu.make_async_copy(w_in_hbm.at[at], w_in.at[at], load_sem.at[5 + c]))
     load_tokens.start()
     load_gain.start()
     load_w[0].start()
-    load_chan.start()
+    load_small.start()
     for load in load_w[1:]:
         load.start()
 
@@ -307,7 +303,6 @@
     for c in range(CHUNKS):
         load_w[c].wait()
         if c == CHUNKS - 1:
-            load_fold.start()
 
             @pl.when(is_host)
             def _():
@@ -319,12 +314,12 @@
         )
         mixin = (mixin * factor).astype(jnp.bfloat16)
         if c == 0:
-            load_chan.wait()
+            load_small.wait()
         for i in range(size // GROUP_CH):
             g = c * (size // GROUP_CH) + i
             first_out[g] = jnp.dot(
                 mixin[:, i * GROUP_CH : (i + 1) * GROUP_CH],
-                chan[...],
+                small[0],
                 preferred_element_type=jnp.float32,
             ).astype(jnp.bfloat16)
             if g == 0:
@@ -337,30 +332,32 @@
                 def _():
                     pl.semaphore_wait(barrier, groups)
 
-            @pl.when(me != hosts[g])
+            spot = hosts[g]
+
+            @pl.when(me != spot)
             def _():
                 pltpu.make_async_remote_copy(
                     src_ref=first_out.at[g],
                     dst_ref=first_in.at[me],
                     send_sem=send_sem.at[0],
                     recv_sem=recv_a.at[0],
-                    device_id=device(hosts[g]),
+                    device_id=device(spot),
                     device_id_type=MESH,
                 ).start()
 
-            @pl.when(me == hosts[g])
+            @pl.when(me == spot)
             def _():
                 first_in[me] = first_out[g]
 
-    load_fold.wait()
     load_out.wait()
     for g in range(groups):
         span = slice(g * GROUP_CH, (g + 1) * GROUP_CH)
-        folded = jnp.dot(fold[...], w_out[span, :], preferred_element_type=jnp.float32)
-        if g < groups - 1:
+        folded = jnp.dot(small[1], w_out[span, :], preferred_element_type=jnp.float32)
+        if g < groups - LATE:
             w_first[span, :] = folded.astype(jnp.bfloat16)
         else:
-            w_last[...] = folded.astype(jnp.bfloat16)
+            at = (g - groups + LATE) * GROUP_CH
+            w_last[at : at + GROUP_CH, :] = folded.astype(jnp.bfloat16)
 
     slots = row_slots(peers)
 
@@ -370,50 +367,46 @@
         rest = first_in.at[pl.ds(0, peers - 1)]
         pltpu.make_async_copy(rest, rest, recv_a.at[0]).wait()
         step = 16
-        cosine_lane = lax.broadcasted_iota(jnp.int32, (step, LANES), 1) <= half
-        for top in range(0, tok_count, step):
-            arrived = [first_in[s, top : top + step].astype(jnp.float32) for s in range(peers)]
-            for a, (cosine, sine) in short_transform(arrived).items():
-                if sine is None:
-                    upper = jnp.where(cosine_lane, cosine, 0.0)
-                    lower = jnp.where(cosine_lane, 0.0, -cosine)
-                else:
-                    upper = jnp.where(cosine_lane, cosine, sine)
-                    lower = jnp.where(cosine_lane, sine, -cosine)
-                blocks[a, top : top + step] = upper.astype(jnp.bfloat16)
-                blocks[a, tok_count + top : tok_count + top + step] = lower.astype(jnp.bfloat16)
-        for i in range(0, peers, 2):
-            pair = [
-                jnp.dot(
-                    mid[a], blocks[min(a, peers - a)], preferred_element_type=jnp.float32
-                ).reshape(peers, fine, LANES)
-                for a in slots[i : i + 2]
-            ]
-            second_out[:, i * fine : (i + 2) * fine, :] = jnp.concatenate(pair, axis=1).astype(
-                jnp.bfloat16
-            )
-
-        def send(target):
-            pltpu.make_async_remote_copy(
-                src_ref=second_out.at[target],
-                dst_ref=second_in.at[group],
-                send_sem=send_sem.at[1],
-                recv_sem=recv_b.at[group],
-                device_id={"row": target // col_count, "col": lax.rem(target, col_count)},
-                device_id_type=MESH,
-            ).start()
-
-        low = spots[0][0]
-        for i in range(low):
-            for edge in (i, row_count - 1 - i):
-                for c in range(col_count):
-                    send(edge * col_count + c)
-        other = low * 2 + 1 - row
-        for c in range(col_count):
-            send(other * col_count + c)
-        for shift in range(1, col_count):
-            send(row * col_count + lax.rem(col + shift, col_count))
-        second_in[group] = second_out[me]
+        cosine_lane = lax.broadcasted_iota(jnp.int16, (step, LANES), 1) <= half
+        zero = jnp.zeros((step, LANES), jnp.bfloat16)
+        for parity, transform in enumerate((even_transform, odd_transform)):
+            for top in range(0, tok_count, step):
+                arrived = [first_in[s, top : top + step] for s in range(peers)]
+                for a, (cosine, sine) in transform(arrived).items():
+                    cosine = cosine.astype(jnp.bfloat16)
+                    sine = zero if sine is None else sine.astype(jnp.bfloat16)
+                    blocks[a, top : top + step] = jnp.where(cosine_lane, cosine, sine)
+                    blocks[a, tok_count + top : tok_count + top + step] = jnp.where(
+                        cosine_lane, sine, -cosine
+                    )
+            for i in range(parity * peers // 2, (parity + 1) * peers // 2, 2):
+                pair = [
+                    jnp.dot(
+                        mid[i + n], blocks[min(a, peers - a)], preferred_element_type=jnp.float32
+                    ).reshape(peers, fine, LANES)
+                    for n, a in enumerate(slots[i : i + 2])
+                ]
+                second_out[:, i * fine : (i + 2) * fine, :] = jnp.concatenate(pair, axis=1).astype(
+                    jnp.bfloat16
+                )
+
+    served = [0, row_count - 1, *range(1, row_count - 1)]
+    served = [r * col_count + c for r in served for c in range(col_count)]
+    for g, spot in enumerate(hosts):
+
+        @pl.when(me == spot)
+        def _():
+            for target in served:
+                if target != spot:
+                    pltpu.make_async_remote_copy(
+                        src_ref=second_out.at[target],
+                        dst_ref=second_in.at[g],
+                        send_sem=send_sem.at[1],
+                        recv_sem=recv_b.at[g // LATE],
+                        device_id=device(target),
+                        device_id_type=MESH,
+                    ).start()
+            second_in[g] = second_out[spot]
 
     @pl.when(is_host)
     def _():
@@ -426,11 +419,20 @@
 
     flipped = jnp.where(lax.broadcasted_iota(jnp.int32, (fine, LANES), 1) > half, -1.0, 1.0)
 
+    def arrive(pair):
+        own = (me == hosts[pair * LATE]) | (me == hosts[pair * LATE + 1])
+
+        @pl.when(own)
+        def _():
+            one = second_in.at[pair * LATE]
+            pltpu.make_async_copy(one, one, recv_b.at[pair]).wait()
+
+        @pl.when(jnp.logical_not(own))
+        def _():
+            both = second_in.at[pl.ds(pair * LATE, LATE)]
+            pltpu.make_async_copy(both, both, recv_b.at[pair]).wait()
+
     def collect(g):
-        @pl.when(me != hosts[g])
-        def _():
-            pltpu.make_async_copy(second_in.at[g], second_in.at[g], recv_b.at[g]).wait()
-
         for i, a in enumerate(slots):
             part = second_in[g, i * fine : (i + 1) * fine].astype(jnp.float32)
             if a > peers // 2:
@@ -438,26 +440,19 @@
             natural[g, pl.ds(a, fine, stride=peers), :] = part
         return natural[g].astype(jnp.bfloat16)
 
-    def project(g, value):
-        return jnp.dot(
-            value,
-            w_first[g * GROUP_CH : (g + 1) * GROUP_CH, :],
-            preferred_element_type=jnp.float32,
-        )
-
-    for g in range(groups - 1):
-        term = project(g, collect(g))
-        if g == 0:
-            partial_ref[...] = term
-        else:
-            partial_ref[...] += term
+    arrive(0)
+    early = [collect(g) for g in range(LATE)]
+    partial_ref[...] = jnp.dot(
+        jnp.concatenate(early, axis=1), w_first[...], preferred_element_type=jnp.float32
+    )
+    arrive(1)
+    for g in range(LATE):
+        last_ref[:, g * GROUP_CH : (g + 1) * GROUP_CH] = collect(LATE + g)
 
     @pl.when(is_host)
     def _():
         sent = second_out.at[pl.ds(0, peers - 1)]
         pltpu.make_async_copy(sent, sent, send_sem.at[1]).wait()
-
-    last_ref[...] = collect(groups - 1)
 
 
 def project_kernel(chunks, last, partial, w_last, out_hbm, staged, sem):
@@ -485,25 +480,25 @@
     last, partial, w_last = pl.pallas_call(
         functools.partial(fused_kernel, shape),
         out_shape=(
-            pltpu.VMEM((tok_count, GROUP_CH), jnp.bfloat16),
+            pltpu.VMEM((tok_count, LATE * GROUP_CH), jnp.bfloat16),
             pltpu.VMEM((tok_count, width), jnp.float32),
-            pltpu.VMEM((GROUP_CH, width), jnp.bfloat16),
+            pltpu.VMEM((LATE * GROUP_CH, width), jnp.bfloat16),
         ),
         in_specs=[pl.BlockSpec(memory_space=pltpu.HBM)] * len(operands),
         out_specs=(pl.BlockSpec(memory_space=pltpu.VMEM),) * 3,
         scratch_shapes=held
         + [
-            pltpu.VMEM((feat_count - GROUP_CH, width), jnp.bfloat16),
+            pltpu.VMEM((feat_count - LATE * GROUP_CH, width), jnp.bfloat16),
             pltpu.VMEM((groups, tok_count, GROUP_CH), jnp.float32),
             pltpu.VMEM((groups, tok_count, GROUP_CH), jnp.bfloat16),
             pltpu.VMEM((peers, tok_count, GROUP_CH), jnp.bfloat16),
             pltpu.VMEM((peers // 2 + 1, 2 * tok_count, GROUP_CH), jnp.bfloat16),
             pltpu.VMEM((peers, tok_count, GROUP_CH), jnp.bfloat16),
             pltpu.VMEM((groups, tok_count, GROUP_CH), jnp.bfloat16),
-            pltpu.SemaphoreType.DMA((6 + CHUNKS,)),
+            pltpu.SemaphoreType.DMA((5 + CHUNKS,)),
             pltpu.SemaphoreType.DMA((2,)),
             pltpu.SemaphoreType.DMA((1,)),
-            pltpu.SemaphoreType.DMA((groups,)),
+            pltpu.SemaphoreType.DMA((groups // LATE,)),
         ],
         compiler_params=pltpu.CompilerParams(
             collective_id=0, has_side_effects=True, vmem_limit_bytes=62_000_000

time: 15.4 us -> 15.2 us (0.987)
  Pallas kernels: 15.2 us -> 15 us
    pallas_call x1, Pallas kernels: 14.3 us -> 14 us  [fused_shards(): pl.pallas_call(functools.partial(fused_kernel, shape), out_shape=(pltpu.V...]
where the time goes in v3:
time: 15.2 us; the launch traced here: 15 us
  Pallas kernels  15 us (99%)
    pallas_call x1, Pallas kernels, fused_shards(): pl.pallas_call(functools.partial(fused_kernel, shape), out_shape=(pltpu.V...  14 us
    pallas_call x1, Pallas kernels, fused_shards(): pl.pallas_call(functools.partial(project_kernel, pieces), out_shape=jax.S...  1.01 us

profile of v3, /device:TPU:0, one launch (start us, length us, event | category | flops | bytes accessed | tf_op | source)
XLA Modules:
  0.0 15.0 jit_solution(12521453746200486501)
XLA Ops:
  0.0 14.0 %shard_map.64 = (bf16[128,256]{1,0:T(8,128)(2,1)S(1)}, f32[128,2048]{1,0:T(8,128)S(1)}, bf16[256,2048]{1,0:T(8,128)(2,1)S(1)}) custom-call(bf16[128,2048]{1,0:T(8,128)(2,1)} %bitcast.2, bf16[2048]{0:T(1024)(128)(2,1)} %gain_hbm.1, bf16[2048,512]{1,0:T(8,128)(2,1)} %w_in_hbm.1, bf16[2,128,128]{2,1,0:T(8,128)(2,1)} %constant.4.clone.small_hbm, ...), custom_call_target="tpu_custom_call" | custom-call | tf_op jit(solution)/shard_map/pallas_call | solution.py:480
  14.0 1.0 %shard_map.65 = bf16[128,2048]{1,0:T(8,128)(2,1)} custom-call(bf16[128,256]{1,0:T(8,128)(2,1)S(1)} %get-tuple-element.8.last, f32[128,2048]{1,0:T(8,128)S(1)} %get-tuple-element.9.partial, bf16[256,2048]{1,0:T(8,128)(2,1)S(1)} %get-tuple-element.10.w_last), custom_call_target="tpu_custom_call" | custom-call | tf_op jit(solution)/shard_map/pallas_call | solution.py:508

commit v4 on v3

--- a/solution.py
+++ b/solution.py
@@ -127,7 +127,7 @@
     return mixed.reshape(seq_count, fine_count * row_count, width)
 
 
-CHUNKS = 4
+CHUNKS = (1, 3)
 LATE = 2
 LANES = 128
 MESH = pl.DeviceIdType.MESH
@@ -182,40 +182,62 @@
     return [jnp.asarray(x, jnp.bfloat16) for x in (np.stack([chan, fold]), mid)]
 
 
+def plus(a, b):
+    if a is None or b is None:
+        return b if a is None else a
+    return a + b
+
+
+def minus(a, b):
+    if a is None or b is None:
+        return a if b is None else -b
+    return a - b
+
+
+def times(a, factor):
+    return None if a is None else a * factor
+
+
+def widen(a):
+    return None if a is None else a.astype(jnp.float32)
+
+
 def even_transform(x):
     r = math.sqrt(0.5)
-    e = [(x[s] + x[s + 8]).astype(jnp.float32) for s in range(8)]
-    p04, n04 = e[0] + e[4], e[0] - e[4]
-    p26, n26 = e[2] + e[6], e[2] - e[6]
-    p15, n15 = e[1] + e[5], e[1] - e[5]
-    p37, n37 = e[3] + e[7], e[3] - e[7]
-    low, high = p04 + p26, p15 + p37
-    even_cos = (n15 - n37) * r
-    even_sin = (n15 + n37) * r
+    e = [widen(plus(x[s], x[s + 8])) for s in range(8)]
+    p04, n04 = plus(e[0], e[4]), minus(e[0], e[4])
+    p26, n26 = plus(e[2], e[6]), minus(e[2], e[6])
+    p15, n15 = plus(e[1], e[5]), minus(e[1], e[5])
+    p37, n37 = plus(e[3], e[7]), minus(e[3], e[7])
+    low, high = plus(p04, p26), plus(p15, p37)
+    even_cos = times(minus(n15, n37), r)
+    even_sin = times(plus(n15, n37), r)
     return {
-        0: (low + high, None),
-        8: (low - high, None),
-        4: (p04 - p26, p15 - p37),
-        2: (n04 + even_cos, even_sin + n26),
-        6: (n04 - even_cos, even_sin - n26),
+        0: (plus(low, high), None),
+        8: (minus(low, high), None),
+        4: (minus(p04, p26), minus(p15, p37)),
+        2: (plus(n04, even_cos), plus(even_sin, n26)),
+        6: (minus(n04, even_cos), minus(even_sin, n26)),
     }
 
 
 def odd_transform(x):
     r = math.sqrt(0.5)
     c1, s1 = math.cos(math.pi / 8), math.sin(math.pi / 8)
-    o = [(x[s] - x[s + 8]).astype(jnp.float32) for s in range(8)]
-    f1, f2, f3 = o[1] - o[7], (o[2] - o[6]) * r, o[3] - o[5]
-    g1, g2, g3 = o[1] + o[7], (o[2] + o[6]) * r, o[3] + o[5]
-    up, down = o[0] + f2, o[0] - f2
-    one, two = f1 * c1 + f3 * s1, f1 * s1 - f3 * c1
-    plus, minus = g2 + o[4], g2 - o[4]
-    three, four = g1 * s1 + g3 * c1, g1 * c1 - g3 * s1
+    o = [widen(minus(x[s], x[s + 8])) for s in range(8)]
+    f1, f2, f3 = minus(o[1], o[7]), times(minus(o[2], o[6]), r), minus(o[3], o[5])
+    g1, g2, g3 = plus(o[1], o[7]), times(plus(o[2], o[6]), r), plus(o[3], o[5])
+    up, down = plus(o[0], f2), minus(o[0], f2)
+    one = plus(times(f1, c1), times(f3, s1))
+    two = minus(times(f1, s1), times(f3, c1))
+    add, sub = plus(g2, o[4]), minus(g2, o[4])
+    three = plus(times(g1, s1), times(g3, c1))
+    four = minus(times(g1, c1), times(g3, s1))
     return {
-        1: (up + one, three + plus),
-        7: (up - one, three - plus),
-        3: (down + two, four + minus),
-        5: (down - two, four - minus),
+        1: (plus(up, one), plus(three, add)),
+        7: (minus(up, one), minus(three, add)),
+        3: (plus(down, two), plus(four, sub)),
+        5: (minus(down, two), minus(four, sub)),
     }
 
 
@@ -243,6 +265,7 @@
     blocks,
     second_out,
     second_in,
+    early,
     load_sem,
     send_sem,
     recv_a,
@@ -270,10 +293,13 @@
     load_small = pltpu.make_async_copy(small_hbm, small, load_sem.at[2])
     load_mid = pltpu.make_async_copy(mid_hbm, mid, load_sem.at[3])
     load_out = pltpu.make_async_copy(w_out_hbm, w_out, load_sem.at[4])
-    size = feat_count // CHUNKS
+    edges = [sum(CHUNKS[:c]) for c in range(len(CHUNKS) + 1)]
+    spans = [
+        (edges[c] * GROUP_CH, (edges[c + 1] - edges[c]) * GROUP_CH) for c in range(len(CHUNKS))
+    ]
     load_w = []
-    for c in range(CHUNKS):
-        at = (slice(None), pl.ds(c * size, size))
+    for c, (left, size) in enumerate(spans):
+        at = (slice(None), pl.ds(left, size))
         load_w.append(pltpu.make_async_copy(w_in_hbm.at[at], w_in.at[at], load_sem.at[5 + c]))
     load_tokens.start()
     load_gain.start()
@@ -300,9 +326,9 @@
     scaled = tokens[...] * gain[...].reshape(1, width)
     widened = tokens[...].astype(jnp.float32)
     factor = lax.rsqrt(jnp.mean(widened * widened, -1, keepdims=True) + NORM_EPS)
-    for c in range(CHUNKS):
+    for c, (left, size) in enumerate(spans):
         load_w[c].wait()
-        if c == CHUNKS - 1:
+        if c == len(spans) - 1:
 
             @pl.when(is_host)
             def _():
@@ -310,28 +336,27 @@
 
             load_out.start()
         mixin = jnp.dot(
-            scaled, w_in[:, c * size : (c + 1) * size], preferred_element_type=jnp.float32
+            scaled, w_in[:, left : left + size], preferred_element_type=jnp.float32
         )
         mixin = (mixin * factor).astype(jnp.bfloat16)
         if c == 0:
             load_small.wait()
-        for i in range(size // GROUP_CH):
-            g = c * (size // GROUP_CH) + i
+        for g in range(edges[c], edges[c + 1]):
+            at = g * GROUP_CH - left
             first_out[g] = jnp.dot(
-                mixin[:, i * GROUP_CH : (i + 1) * GROUP_CH],
-                small[0],
-                preferred_element_type=jnp.float32,
+                mixin[:, at : at + GROUP_CH], small[0], preferred_element_type=jnp.float32
             ).astype(jnp.bfloat16)
-            if g == 0:
-
-                @pl.when(is_host)
-                def _():
-                    pl.semaphore_wait(barrier, groups - 1)
-
-                @pl.when(jnp.logical_not(is_host))
-                def _():
-                    pl.semaphore_wait(barrier, groups)
-
+        if c == 0:
+
+            @pl.when(is_host)
+            def _():
+                pl.semaphore_wait(barrier, groups - 1)
+
+            @pl.when(jnp.logical_not(is_host))
+            def _():
+                pl.semaphore_wait(barrier, groups)
+
+        for g in range(edges[c], edges[c + 1]):
             spot = hosts[g]
 
             @pl.when(me != spot)
@@ -340,7 +365,7 @@
                     src_ref=first_out.at[g],
                     dst_ref=first_in.at[me],
                     send_sem=send_sem.at[0],
-                    recv_sem=recv_a.at[0],
+                    recv_sem=recv_a.at[jnp.where(row == row_count - 1, 1, 0)],
                     device_id=device(spot),
                     device_id_type=MESH,
                 ).start()
@@ -364,15 +389,30 @@
     @pl.when(is_host)
     def _():
         load_mid.wait()
-        rest = first_in.at[pl.ds(0, peers - 1)]
+        step = 16
+        late_count = col_count
+        late_top = peers - late_count
+        rest = first_in.at[pl.ds(0, late_top - 1)]
         pltpu.make_async_copy(rest, rest, recv_a.at[0]).wait()
-        step = 16
+        for transform in (even_transform, odd_transform):
+            for top in range(0, tok_count, step):
+                rows = slice(top, top + step)
+                arrived = [first_in[s, rows] for s in range(late_top)] + [None] * late_count
+                for a, (cosine, sine) in transform(arrived).items():
+                    early[a, 0, rows] = cosine
+                    if sine is not None:
+                        early[a, 1, rows] = sine
+        rest = first_in.at[pl.ds(0, late_count)]
+        pltpu.make_async_copy(rest, rest, recv_a.at[1]).wait()
         cosine_lane = lax.broadcasted_iota(jnp.int16, (step, LANES), 1) <= half
         zero = jnp.zeros((step, LANES), jnp.bfloat16)
         for parity, transform in enumerate((even_transform, odd_transform)):
             for top in range(0, tok_count, step):
-                arrived = [first_in[s, top : top + step] for s in range(peers)]
+                rows = slice(top, top + step)
+                arrived = [None] * late_top + [first_in[s, rows] for s in range(late_top, peers)]
                 for a, (cosine, sine) in transform(arrived).items():
+                    cosine = plus(early[a, 0, rows], cosine)
+                    sine = None if sine is None else plus(early[a, 1, rows], sine)
                     cosine = cosine.astype(jnp.bfloat16)
                     sine = zero if sine is None else sine.astype(jnp.bfloat16)
                     blocks[a, top : top + step] = jnp.where(cosine_lane, cosine, sine)
@@ -441,9 +481,9 @@
         return natural[g].astype(jnp.bfloat16)
 
     arrive(0)
-    early = [collect(g) for g in range(LATE)]
+    values = [collect(g) for g in range(LATE)]
     partial_ref[...] = jnp.dot(
-        jnp.concatenate(early, axis=1), w_first[...], preferred_element_type=jnp.float32
+        jnp.concatenate(values, axis=1), w_first[...], preferred_element_type=jnp.float32
     )
     arrive(1)
     for g in range(LATE):
@@ -495,9 +535,10 @@
             pltpu.VMEM((peers // 2 + 1, 2 * tok_count, GROUP_CH), jnp.bfloat16),
             pltpu.VMEM((peers, tok_count, GROUP_CH), jnp.bfloat16),
             pltpu.VMEM((groups, tok_count, GROUP_CH), jnp.bfloat16),
-            pltpu.SemaphoreType.DMA((5 + CHUNKS,)),
+            pltpu.VMEM((peers // 2 + 1, 2, tok_count, GROUP_CH), jnp.float32),
+            pltpu.SemaphoreType.DMA((5 + len(CHUNKS),)),
             pltpu.SemaphoreType.DMA((2,)),
-            pltpu.SemaphoreType.DMA((1,)),
+            pltpu.SemaphoreType.DMA((2,)),
             pltpu.SemaphoreType.DMA((groups // LATE,)),
         ],
         compiler_params=pltpu.CompilerParams(

time: 15.2 us -> 15.2 us (level)
  no operation moved by 1% of the time
where the time goes in v4:
time: 15.2 us; the launch traced here: 15 us
  Pallas kernels  15 us (99%)
    pallas_call x1, Pallas kernels, fused_shards(): pl.pallas_call(functools.partial(fused_kernel, shape), out_shape=(pltpu.V...  14 us
    pallas_call x1, Pallas kernels, fused_shards(): pl.pallas_call(functools.partial(project_kernel, pieces), out_shape=jax.S...  1 us

profile of v4, /device:TPU:0, one launch (start us, length us, event | category | flops | bytes accessed | tf_op | source)
XLA Modules:
  0.0 15.0 jit_solution(1557693215692208248)
XLA Ops:
  0.0 14.0 %shard_map.64 = (bf16[128,256]{1,0:T(8,128)(2,1)S(1)}, f32[128,2048]{1,0:T(8,128)S(1)}, bf16[256,2048]{1,0:T(8,128)(2,1)S(1)}) custom-call(bf16[128,2048]{1,0:T(8,128)(2,1)} %bitcast.2, bf16[2048]{0:T(1024)(128)(2,1)} %gain_hbm.1, bf16[2048,512]{1,0:T(8,128)(2,1)} %w_in_hbm.1, bf16[2,128,128]{2,1,0:T(8,128)(2,1)} %constant.4.clone.small_hbm, ...), custom_call_target="tpu_custom_call" | custom-call | tf_op jit(solution)/shard_map/pallas_call | solution.py:520
  14.0 1.0 %shard_map.65 = bf16[128,2048]{1,0:T(8,128)(2,1)} custom-call(bf16[128,256]{1,0:T(8,128)(2,1)S(1)} %get-tuple-element.8.last, f32[128,2048]{1,0:T(8,128)S(1)} %get-tuple-element.9.partial, bf16[256,2048]{1,0:T(8,128)(2,1)S(1)} %get-tuple-element.10.w_last), custom_call_target="tpu_custom_call" | custom-call | tf_op jit(solution)/shard_map/pallas_call | solution.py:549

commit v5 on v4

--- a/solution.py
+++ b/solution.py
@@ -282,8 +282,10 @@
     row, col = lax.axis_index("row"), lax.axis_index("col")
     me = row * col_count + col
     is_host = me == hosts[0]
-    for spot in hosts[1:]:
-        is_host = is_host | (me == spot)
+    group = jnp.int32(0)
+    for g in range(1, groups):
+        is_host = is_host | (me == hosts[g])
+        group = group + jnp.where(me == hosts[g], g, 0)
 
     def device(index):
         return {"row": index // col_count, "col": index % col_count}
@@ -419,18 +421,32 @@
                     blocks[a, tok_count + top : tok_count + top + step] = jnp.where(
                         cosine_lane, sine, -cosine
                     )
-            for i in range(parity * peers // 2, (parity + 1) * peers // 2, 2):
-                pair = [
-                    jnp.dot(
-                        mid[i + n], blocks[min(a, peers - a)], preferred_element_type=jnp.float32
-                    ).reshape(peers, fine, LANES)
-                    for n, a in enumerate(slots[i : i + 2])
-                ]
-                second_out[:, i * fine : (i + 2) * fine, :] = jnp.concatenate(pair, axis=1).astype(
-                    jnp.bfloat16
-                )
-
-    served = [0, row_count - 1, *range(1, row_count - 1)]
+            cuts = (0, peers) if parity == 0 else (0, col_count, peers)
+            for first, stop in zip(cuts, cuts[1:]):
+                for i in range(parity * peers // 2, (parity + 1) * peers // 2, 2):
+                    pair = [
+                        jnp.dot(
+                            mid[i + n, first * fine : stop * fine],
+                            blocks[min(a, peers - a)],
+                            preferred_element_type=jnp.float32,
+                        ).reshape(stop - first, fine, LANES)
+                        for n, a in enumerate(slots[i : i + 2])
+                    ]
+                    second_out[first:stop, i * fine : (i + 2) * fine, :] = jnp.concatenate(
+                        pair, axis=1
+                    ).astype(jnp.bfloat16)
+                if stop == col_count:
+                    for target in range(col_count):
+                        pltpu.make_async_remote_copy(
+                            src_ref=second_out.at[target],
+                            dst_ref=second_in.at[group],
+                            send_sem=send_sem.at[1],
+                            recv_sem=recv_b.at[group // LATE],
+                            device_id=device(target),
+                            device_id_type=MESH,
+                        ).start()
+
+    served = [row_count - 1, *range(1, row_count - 1)]
     served = [r * col_count + c for r in served for c in range(col_count)]
     for g, spot in enumerate(hosts):
 

time: 15.2 us -> 15.1 us (level)
  no operation moved by 1% of the time
where the time goes in v5:
time: 15.1 us; the launch traced here: 15 us
  Pallas kernels  15 us (99%)
    pallas_call x1, Pallas kernels, fused_shards(): pl.pallas_call(functools.partial(fused_kernel, shape), out_shape=(pltpu.V...  13.9 us
    pallas_call x1, Pallas kernels, fused_shards(): pl.pallas_call(functools.partial(project_kernel, pieces), out_shape=jax.S...  1.01 us

profile of v5, /device:TPU:0, one launch (start us, length us, event | category | flops | bytes accessed | tf_op | source)
XLA Modules:
  0.0 15.0 jit_solution(2832061067385716342)
XLA Ops:
  0.0 13.9 %shard_map.64 = (bf16[128,256]{1,0:T(8,128)(2,1)S(1)}, f32[128,2048]{1,0:T(8,128)S(1)}, bf16[256,2048]{1,0:T(8,128)(2,1)S(1)}) custom-call(bf16[128,2048]{1,0:T(8,128)(2,1)} %bitcast.2, bf16[2048]{0:T(1024)(128)(2,1)} %gain_hbm.1, bf16[2048,512]{1,0:T(8,128)(2,1)} %w_in_hbm.1, bf16[2,128,128]{2,1,0:T(8,128)(2,1)} %constant.4.clone.small_hbm, ...), custom_call_target="tpu_custom_call" | custom-call | tf_op jit(solution)/shard_map/pallas_call | solution.py:536
  14.0 1.0 %shard_map.65 = bf16[128,2048]{1,0:T(8,128)(2,1)} custom-call(bf16[128,256]{1,0:T(8,128)(2,1)S(1)} %get-tuple-element.8.last, f32[128,2048]{1,0:T(8,128)S(1)} %get-tuple-element.9.partial, bf16[256,2048]{1,0:T(8,128)(2,1)S(1)} %get-tuple-element.10.w_last), custom_call_target="tpu_custom_call" | custom-call | tf_op jit(solution)/shard_map/pallas_call | solution.py:565

commit v6 on v5

--- a/solution.py
+++ b/solution.py
@@ -421,7 +421,7 @@
                     blocks[a, tok_count + top : tok_count + top + step] = jnp.where(
                         cosine_lane, sine, -cosine
                     )
-            cuts = (0, peers) if parity == 0 else (0, col_count, peers)
+            cuts = (0, peers) if parity == 0 else (0, col_count // 2, peers)
             for first, stop in zip(cuts, cuts[1:]):
                 for i in range(parity * peers // 2, (parity + 1) * peers // 2, 2):
                     pair = [
@@ -435,8 +435,8 @@
                     second_out[first:stop, i * fine : (i + 2) * fine, :] = jnp.concatenate(
                         pair, axis=1
                     ).astype(jnp.bfloat16)
-                if stop == col_count:
-                    for target in range(col_count):
+                if stop == col_count // 2:
+                    for target in range(col_count // 2):
                         pltpu.make_async_remote_copy(
                             src_ref=second_out.at[target],
                             dst_ref=second_in.at[group],
@@ -446,8 +446,8 @@
                             device_id_type=MESH,
                         ).start()
 
-    served = [row_count - 1, *range(1, row_count - 1)]
-    served = [r * col_count + c for r in served for c in range(col_count)]
+    served = [0, row_count - 1, *range(1, row_count - 1)]
+    served = [r * col_count + c for r in served for c in range(col_count)][col_count // 2 :]
     for g, spot in enumerate(hosts):
 
         @pl.when(me == spot)

time: 15.1 us -> 15.1 us (level)
  no operation moved by 1% of the time
where the time goes in v6:
time: 15.1 us; the launch traced here: 14.9 us
  Pallas kernels  14.9 us (99%)
    pallas_call x1, Pallas kernels, fused_shards(): pl.pallas_call(functools.partial(fused_kernel, shape), out_shape=(pltpu.V...  13.9 us
    pallas_call x1, Pallas kernels, fused_shards(): pl.pallas_call(functools.partial(project_kernel, pieces), out_shape=jax.S...  1.01 us

profile of v6, /device:TPU:0, one launch (start us, length us, event | category | flops | bytes accessed | tf_op | source)
XLA Modules:
  0.0 14.9 jit_solution(11985969693517431806)
XLA Ops:
  0.0 13.9 %shard_map.64 = (bf16[128,256]{1,0:T(8,128)(2,1)S(1)}, f32[128,2048]{1,0:T(8,128)S(1)}, bf16[256,2048]{1,0:T(8,128)(2,1)S(1)}) custom-call(bf16[128,2048]{1,0:T(8,128)(2,1)} %bitcast.2, bf16[2048]{0:T(1024)(128)(2,1)} %gain_hbm.1, bf16[2048,512]{1,0:T(8,128)(2,1)} %w_in_hbm.1, bf16[2,128,128]{2,1,0:T(8,128)(2,1)} %constant.4.clone.small_hbm, ...), custom_call_target="tpu_custom_call" | custom-call | tf_op jit(solution)/shard_map/pallas_call | solution.py:536
  13.9 1.0 %shard_map.65 = bf16[128,2048]{1,0:T(8,128)(2,1)} custom-call(bf16[128,256]{1,0:T(8,128)(2,1)S(1)} %get-tuple-element.8.last, f32[128,2048]{1,0:T(8,128)S(1)} %get-tuple-element.9.partial, bf16[256,2048]{1,0:T(8,128)(2,1)S(1)} %get-tuple-element.10.w_last), custom_call_target="tpu_custom_call" | custom-call | tf_op jit(solution)/shard_map/pallas_call | solution.py:565

commit v7 on v5

--- a/solution.py
+++ b/solution.py
@@ -561,7 +561,7 @@
             collective_id=0, has_side_effects=True, vmem_limit_bytes=62_000_000
         ),
     )(*operands)
-    pieces = max(1, width // 512)
+    pieces = max(1, width // 256)
     mixed = pl.pallas_call(
         functools.partial(project_kernel, pieces),
         out_shape=jax.ShapeDtypeStruct((tok_count, width), jnp.bfloat16),

time: 15.1 us -> 15.1 us (level)
  no operation moved by 1% of the time
where the time goes in v7:
time: 15.1 us; the launch traced here: 15 us
  Pallas kernels  14.9 us (99%)
    pallas_call x1, Pallas kernels, fused_shards(): pl.pallas_call(functools.partial(fused_kernel, shape), out_shape=(pltpu.V...  13.9 us
    pallas_call x1, Pallas kernels, fused_shards(): pl.pallas_call(functools.partial(project_kernel, pieces), out_shape=jax.S...  1 us

profile of v7, /device:TPU:0, one launch (start us, length us, event | category | flops | bytes accessed | tf_op | source)
XLA Modules:
  0.0 15.0 jit_solution(15191288720943726450)
XLA Ops:
  0.0 13.9 %shard_map.64 = (bf16[128,256]{1,0:T(8,128)(2,1)S(1)}, f32[128,2048]{1,0:T(8,128)S(1)}, bf16[256,2048]{1,0:T(8,128)(2,1)S(1)}) custom-call(bf16[128,2048]{1,0:T(8,128)(2,1)} %bitcast.2, bf16[2048]{0:T(1024)(128)(2,1)} %gain_hbm.1, bf16[2048,512]{1,0:T(8,128)(2,1)} %w_in_hbm.1, bf16[2,128,128]{2,1,0:T(8,128)(2,1)} %constant.4.clone.small_hbm, ...), custom_call_target="tpu_custom_call" | custom-call | tf_op jit(solution)/shard_map/pallas_call | solution.py:536
  14.0 1.0 %shard_map.65 = bf16[128,2048]{1,0:T(8,128)(2,1)} custom-call(bf16[128,256]{1,0:T(8,128)(2,1)S(1)} %get-tuple-element.8.last, f32[128,2048]{1,0:T(8,128)S(1)} %get-tuple-element.9.partial, bf16[256,2048]{1,0:T(8,128)(2,1)S(1)} %get-tuple-element.10.w_last), custom_call_target="tpu_custom_call" | custom-call | tf_op jit(solution)/shard_map/pallas_call | solution.py:565
